TPU v7x, 256 devices: a whole 4x4x8 slice. The times are simulated.
256 devices in a mesh: sp: 64 (over z, y, core), tp: 4 (over x).
Axes of the slice: x: 4, y: 4, z: 8, core: 2. Of those that a mesh axis runs over, the one named last changes fastest.
Arguments:
- out_grad: bfloat16 [12288, 2048], P('sp'), may hold values from -16 to 16
- routes: int32 [12288, 2], P('sp'), may hold values from 0 to 63, all different within a row; in each aligned block of 192 rows (0 to 191, 192 to 383, ...) at most 12 rows name the same one
- route_weight: float32 [12288, 2], P('sp'), may hold values from 0.3 to 1.5
- expert_rows: bfloat16 [64, 64, 12, 2048], P(None, 'sp'), may hold values from -6 to 6
- gate_weight: bfloat16 [64, 2048, 1024], P('sp', None, 'tp'), may hold values from -0.125 to 0.125
- up_weight: bfloat16 [64, 2048, 1024], P('sp', None, 'tp'), may hold values from -0.125 to 0.125
- down_weight: bfloat16 [64, 1024, 2048], P('sp', 'tp'), may hold values from -0.1875 to 0.1875
- conv_input: bfloat16 [12288, 1024], P('sp', 'tp'), may hold values from -6 to 6
- out_gate: bfloat16 [12288, 1024], P('sp', 'tp'), may hold values from -6 to 6
- in_gate: bfloat16 [12288, 1024], P('sp', 'tp'), may hold values from -6 to 6
- taps: float32 [3, 1024], P(None, 'tp'), may hold values from -3 to 3
- out_weight: bfloat16 [2048, 1024], P(None, 'tp'), may hold values from -0.1875 to 0.1875
Outputs:
- gate_grad: bfloat16 [64, 2048, 1024], P('sp', None, 'tp')
- up_grad: bfloat16 [64, 2048, 1024], P('sp', None, 'tp')
- down_grad: bfloat16 [64, 1024, 2048], P('sp', 'tp')
- mid_grad: bfloat16 [12288, 2048], P('sp', 'tp')
- out_weight_grad: float32 [2048, 1024], P('sp', 'tp')
- input_grad: bfloat16 [12288, 1024], P('sp', 'tp')
- out_gate_grad: bfloat16 [12288, 1024], P('sp', 'tp')
- in_gate_grad: bfloat16 [12288, 1024], P('sp', 'tp')
Inputs may be any that keep to these rules, and one draw needn't show every extreme that they name: `routes`: each token names 2 different experts; within each aligned block of 192 tokens no expert is named by more than 12 tokens, a bound that some block reaches.
All inputs are finite; a program needn't handle non-finite values.
Results may differ from a plain program's by a relative error of at most 0.014.
Values may be sent and summed in bfloat16 or wider, within the bound.
No kernel may reach another device: no remote copies, remote signals or barrier semaphores. Data moves between devices by JAX's collectives and lax.ppermute only.
A program may use at most 64 MiB of HBM per device.

v0:
```python
import jax
import jax.numpy as jnp
from jax import lax
from jax.experimental import pallas as pl
from jax.experimental.pallas import tpu as pltpu
from jax.sharding import PartitionSpec as P


F32 = jnp.float32
BF16 = jnp.bfloat16


def mm(a, b, contract):
    return lax.dot_general(a, b, ((contract[0], contract[1]), ((), ())), preferred_element_type=F32)


def slot_hits(routes_ref, slots, rows):
    tokens = routes_ref.shape[1]
    row = lax.broadcasted_iota(jnp.int32, (rows, tokens), 0)
    expert = lax.shift_right_logical(row * ((1 << 17) // slots + 1), 17)
    slot = row - expert * slots
    first = routes_ref[0:1, :] == expert
    second = routes_ref[1:2, :] == expert
    named = jnp.where(first | second, 1.0, 0.0)
    sooner = lax.broadcasted_iota(jnp.int32, (tokens, tokens), 0)
    later = lax.broadcasted_iota(jnp.int32, (tokens, tokens), 1)
    order = jnp.where(sooner < later, 1.0, 0.0).astype(BF16)
    place = mm(named.astype(BF16), order, ((1,), (0,)))
    return first, named, place, slot.astype(F32)


def send_kernel(
    first_ref, routes_hbm, weight_hbm, tokens_hbm,
    out_ref, wide_ref, routes_ref, weight_ref, tokens_ref, sems,
):
    loads = [
        pltpu.make_async_copy(routes_hbm, routes_ref, sems.at[0]),
        pltpu.make_async_copy(weight_hbm, weight_ref, sems.at[1]),
        pltpu.make_async_copy(tokens_hbm, tokens_ref, sems.at[2]),
    ]
    for load in loads:
        load.start()
    loads[0].wait()
    loads[1].wait()
    rows = out_ref.shape[0] // (tokens_ref.shape[1] // 128)
    portion = rows // 64
    first, named, place, slot = slot_hits(routes_ref, portion, rows)
    base = first_ref[0].astype(F32)
    hit = jnp.where(place == slot + base, named, 0.0)
    weight = hit * jnp.where(first, weight_ref[0:1, :], weight_ref[1:2, :])
    factor = jnp.sum(weight, axis=1, keepdims=True)
    loads[2].wait()
    picked = mm(hit.astype(BF16), tokens_ref[...], ((1,), (0,))) * factor
    lanes = tokens_ref.shape[1] // 128
    for g in range(lanes):
        wide_ref[pl.ds(g, rows, stride=lanes), :] = picked[:, g * 128 : (g + 1) * 128]
    out_ref[...] = wide_ref[...].astype(BF16)


def arrive_kernel(
    arrived_hbm, w0_hbm, w1_hbm, w2_hbm, w3a_hbm, w3b_hbm,
    rows_ref, p0, p1, p2, p3, wide_ref, arrived_ref, w0, w1, w2, w3, sems,
):
    half = w3a_hbm.shape[0]
    loads = [
        pltpu.make_async_copy(arrived_hbm, arrived_ref, sems.at[0]),
        pltpu.make_async_copy(w3a_hbm, w3.at[pl.ds(0, half), :], sems.at[1]),
        pltpu.make_async_copy(w3b_hbm, w3.at[pl.ds(half, half), :], sems.at[2]),
        pltpu.make_async_copy(w2_hbm, w2, sems.at[3]),
        pltpu.make_async_copy(w1_hbm, w1, sems.at[4]),
        pltpu.make_async_copy(w0_hbm, w0, sems.at[5]),
    ]
    for load in loads:
        load.start()
    loads[0].wait()
    wide_ref[...] = arrived_ref[...].astype(F32)
    sources = 64
    per = arrived_ref.shape[0] // sources
    lanes = rows_ref.shape[1] // 128
    for i in range(per // lanes):
        for g in range(lanes):
            rows_ref[i * sources : (i + 1) * sources, g * 128 : (g + 1) * 128] = wide_ref[
                pl.ds(i * lanes + g, sources, stride=per), :
            ].astype(BF16)
    loads[1].wait()
    loads[2].wait()
    p3[...] = mm(rows_ref[...], w3[...], ((1,), (1,))).astype(BF16)
    for load, w, p in ((loads[3], w2, p2), (loads[4], w1, p1), (loads[5], w0, p0)):
        load.wait()
        p[...] = mm(rows_ref[...], w[...], ((1,), (1,))).astype(BF16)


def row_block(gate_part, up_part, gate_ref, up_ref, which, share):
    span = pl.ds(pl.multiple_of(which * share, share), share)
    block = mm(gate_part, gate_ref[span, :], ((1,), (1,)))
    return block + mm(up_part, up_ref[span, :], ((1,), (1,)))


def parts_kernel(
    member_ref, own, right, far, left, up_of, gate_of, gate_ref, up_ref,
    gate_part, up_part, far_a, far_b,
):
    member = member_ref[0]
    groups = 4
    block = own.shape[0]
    for r, piece in enumerate((own, right, far, left)):
        span = pl.ds(pl.multiple_of(lax.rem(member + r, groups) * block, block), block)
        grad = piece[...].astype(F32)
        up_part[span, :] = (grad * up_of[span, :]).astype(BF16)
        gate_part[span, :] = (grad * gate_of[span, :]).astype(BF16)
    share = far_a.shape[1]
    half = far_a.shape[0]
    which = lax.rem(member + 2, groups)
    part = row_block(gate_part[...], up_part[...], gate_ref, up_ref, which, share).astype(BF16)
    far_a[...] = part[:half]
    far_b[...] = part[half:]


def blocks_kernel(
    member_ref, gate_part, up_part, gate_ref, up_ref,
    next_a, next_b, prev_a, prev_b, own,
):
    member = member_ref[0]
    half, share = next_a.shape
    for by, a, b in ((1, next_a, next_b), (3, prev_a, prev_b)):
        which = lax.rem(member + by, 4)
        part = row_block(gate_part[...], up_part[...], gate_ref, up_ref, which, share)
        a[...] = part[:half].astype(BF16)
        b[...] = part[half:].astype(BF16)
    own[...] = row_block(gate_part[...], up_part[...], gate_ref, up_ref, member, share)


def leave_kernel(own, left_a, right_a, left_b, right_b, out_ref, wide_ref):
    sources = 64
    half, share = left_a.shape
    lanes = share // 128
    per = out_ref.shape[0] // sources
    for p in range(per // lanes):
        left, right = (left_a, right_a) if p * sources < half else (left_b, right_b)
        at = p * sources
        here = at if at < half else at - half
        rows = own[at : at + sources, :]
        rows = rows + left[here : here + sources, :].astype(F32)
        rows = rows + right[here : here + sources, :].astype(F32)
        for g in range(lanes):
            wide_ref[pl.ds(p * lanes + g, sources, stride=per), :] = rows[
                :, g * 128 : (g + 1) * 128
            ]
    out_ref[...] = wide_ref[...].astype(BF16)


def return_kernel(
    core_ref, routes_ref, returned_ref, own_ref, gated_ref,
    mid_ref, sent_ref, kept_ref, wide_ref,
):
    share = mid_ref.shape[1]
    lanes = share // 128
    columns = returned_ref.shape[0] // lanes
    wide_ref[...] = returned_ref[...].astype(F32)
    _, named, place, slot = slot_hits(routes_ref, columns // 64, columns)
    hit = jnp.where(place == slot, named, 0.0).T.astype(BF16)
    for g in range(lanes):
        rows = wide_ref[pl.ds(g, columns, stride=lanes), :].astype(BF16)
        picked = mm(hit, rows, ((1,), (0,)))
        own = own_ref[:, g * 128 : (g + 1) * 128].astype(F32)
        mid_ref[:, g * 128 : (g + 1) * 128] = (own + picked).astype(BF16)
    side = share // 2
    core = core_ref[0]
    for ref, which in ((sent_ref, 1 - core), (kept_ref, core)):
        columns_t = mid_ref[:, pl.ds(pl.multiple_of(which * side, side), side)].T
        for r in range(gated_ref.shape[0]):
            part = mm(columns_t, gated_ref[r], ((1,), (0,)))
            ref[r] = part.astype(ref.dtype)


def down_kernel(act, g0, g1, g2, g3a, g3b, out_ref):
    half = g3a.shape[0]
    total = mm(act[0].T, g0[...], ((1,), (0,)))
    total = total + mm(act[3].T, g1[...], ((1,), (0,)))
    total = total + mm(act[1].T, g2[...], ((1,), (0,)))
    total = total + mm(act[2, :half].T, g3a[...], ((1,), (0,)))
    total = total + mm(act[2, half:].T, g3b[...], ((1,), (0,)))
    out_ref[...] = total.astype(BF16)


def weights_kernel(x_ref, gate_part, up_part, gate_ref, up_ref):
    x = x_ref[...].T
    gate_ref[...] = mm(x, gate_part[...], ((1,), (0,))).astype(BF16)
    up_ref[...] = mm(x, up_part[...], ((1,), (0,))).astype(BF16)


def weight_grads(inputs, gate_part, up_part):
    rows, width = inputs.shape
    hidden = gate_part.shape[1]
    tile = 512
    whole = pl.BlockSpec((rows, hidden), lambda i: (0, 0))
    out = pl.BlockSpec((tile, hidden), lambda i: (i, 0))
    return pl.pallas_call(
        weights_kernel,
        grid=(width // tile,),
        out_shape=[jax.ShapeDtypeStruct((width, hidden), BF16)] * 2,
        in_specs=[pl.BlockSpec((rows, tile), lambda i: (0, i)), whole, whole],
        out_specs=[out, out],
        compiler_params=pltpu.CompilerParams(vmem_limit_bytes=40 << 20),
        name="weights",
    )(inputs, gate_part, up_part)


def call(kernel, outs, scratch, *args, there=False):
    smem = pl.BlockSpec(memory_space=pltpu.SMEM)
    vmem = pl.BlockSpec(memory_space=pltpu.VMEM)
    hbm = pl.BlockSpec(memory_space=pl.ANY)
    return pl.pallas_call(
        kernel,
        out_shape=[jax.ShapeDtypeStruct(*o) for o in outs],
        in_specs=[smem if a.ndim == 1 else hbm if there else vmem for a in args],
        out_specs=[vmem] * len(outs),
        scratch_shapes=scratch,
        compiler_params=pltpu.CompilerParams(vmem_limit_bytes=40 << 20),
    )(*args)


def turn(shard, by):
    peers = lax.axis_size("tp")
    return lax.ppermute(shard, "tp", [(i, (i + by) % peers) for i in range(peers)])


def passed_along(shard, axis, by):
    peers = lax.axis_size(axis)
    pairs = [(i, i + by) for i in range(peers) if 0 <= i + by < peers]
    return lax.ppermute(shard, axis, pairs)


def after(value, *others):
    return lax.optimization_barrier((value, *others))[0]


def gathered(own):
    half = own.shape[0] // 2
    left = turn(own, 1)
    right = turn(own, -1)
    passed_a = left[:half]
    far_a = turn(passed_a, 1)
    passed_b = right[half:]
    far_b = turn(passed_b, -1)
    return (own, left, right, far_a, far_b), (passed_a, passed_b)


def on_device(
    out_grad,
    routes,
    route_weight,
    expert_rows,
    gate_weight,
    up_weight,
    down_weight,
    conv_input,
    out_gate,
    in_gate,
    taps,
    out_weight,
):
    groups = lax.axis_size("tp")
    member = lax.axis_index("tp")
    sources = lax.axis_size("sp")
    tok_rows, width = out_grad.shape
    slots = expert_rows.shape[2]
    share = width // groups
    portion = slots // groups
    experts = sources
    hidden = gate_weight.shape[2]
    rows = slots * sources

    w_down, passed = gathered(down_weight[0])

    packed = portion * width // 128
    (piece,) = call(
        send_kernel,
        [((experts * packed, 128), BF16)],
        [
            pltpu.VMEM((experts * packed, 128), F32),
            pltpu.VMEM(routes.T.shape, jnp.int32),
            pltpu.VMEM(routes.T.shape, F32),
            pltpu.VMEM(out_grad.shape, BF16),
            pltpu.SemaphoreType.DMA((3,)),
        ],
        (member * portion)[None],
        routes.T,
        route_weight.T,
        out_grad,
        there=True,
    )
    arrived = lax.all_to_all(
        piece.reshape(experts, packed, 128), "sp", split_axis=0, concat_axis=0, tiled=True
    )

    in_gate, conv_input, out_gate, early_grad, out_weight = lax.optimization_barrier(
        (in_gate, conv_input, out_gate, out_grad, out_weight, piece, *passed)
    )[:5]
    own_cols = lax.dynamic_slice_in_dim(early_grad, member * share, share, 1)
    reach = taps.shape[0] - 1
    mixed = in_gate.astype(F32) * conv_input.astype(F32)
    prior_mixed = passed_along(mixed[tok_rows - reach :], "sp", 1)
    extended = jnp.concatenate([prior_mixed, mixed], axis=0)
    conv = jnp.zeros_like(mixed)
    for tap in range(reach + 1):
        conv = conv + taps[tap][None, :] * extended[reach - tap : reach - tap + tok_rows]
    gated = (out_gate.astype(F32) * conv).astype(BF16)
    gated_all = jnp.stack([gated, turn(gated, -1), turn(gated, 2), turn(gated, 1)])
    out_weight_twice = jnp.concatenate([out_weight, out_weight], axis=0)
    out_weight_rel = lax.dynamic_slice_in_dim(out_weight_twice, member * share, width, 0)

    inputs = expert_rows[:, 0].transpose(1, 0, 2).reshape(rows, width)
    inputs = after(inputs, *passed)
    gate_w, up_w = gate_weight[0], up_weight[0]
    gate = mm(inputs, gate_w, ((1,), (0,)))
    up = mm(inputs, up_w, ((1,), (0,)))
    sig = jax.nn.sigmoid(gate)
    act = (gate * sig * up).astype(BF16)
    up_of = gate * sig
    gate_of = up * sig * (1.0 + gate * (1.0 - sig))
    act_twice = act.reshape(groups, rows // groups, hidden)
    act_twice = jnp.concatenate([act_twice, act_twice], axis=0)
    act_rel = lax.dynamic_slice_in_dim(act_twice, member, groups, 0)
    (
        arrived, up_of, gate_of, act_rel, gated_all, out_weight_rel, conv, own_cols
    ) = lax.optimization_barrier(
        (arrived, up_of, gate_of, act_rel, gated_all, out_weight_rel, conv, own_cols)
    )

    block = portion * sources
    grads, *partial = call(
        arrive_kernel,
        [((block, width), BF16)] + [((block, hidden), BF16)] * 4,
        [
            pltpu.VMEM((sources * packed, 128), F32),
            pltpu.VMEM((sources * packed, 128), BF16),
            *[pltpu.VMEM((hidden, width), BF16)] * 4,
            pltpu.SemaphoreType.DMA((6,)),
        ],
        arrived.reshape(sources * packed, 128),
        *w_down,
        there=True,
    )
    from_far = turn(partial[3], 2)
    from_left = turn(partial[2], 1)
    from_right = turn(partial[1], -1)
    half = rows // 2
    gate_part, up_part, far_a, far_b = call(
        parts_kernel,
        [((rows, hidden), BF16)] * 2 + [((half, share), BF16)] * 2,
        [],
        member[None],
        partial[0],
        from_right,
        from_far,
        from_left,
        up_of,
        gate_of,
        gate_w,
        up_w,
    )
    far_a = turn(far_a, 1)
    far_b = turn(far_b, -1)
    next_a, next_b, prev_a, prev_b, own = call(
        blocks_kernel,
        [((half, share), BF16)] * 4 + [((rows, share), F32)],
        [],
        member[None],
        gate_part,
        up_part,
        gate_w,
        up_w,
    )
    left_b = turn(next_b, 1)
    right_a = turn(prev_a, -1)
    next_a = (next_a.astype(F32) + far_a.astype(F32)).astype(BF16)
    prev_b = (prev_b.astype(F32) + far_b.astype(F32)).astype(BF16)
    left_a = turn(next_a, 1)
    right_b = turn(prev_b, -1)
    (leaving,) = call(
        leave_kernel,
        [((experts * packed, 128), BF16)],
        [pltpu.VMEM((experts * packed, 128), F32)],
        own,
        left_a,
        right_a,
        left_b,
        right_b,
    )
    returned = lax.all_to_all(
        leaving.reshape(sources, packed, 128), "sp", split_axis=0, concat_axis=0, tiled=True
    )

    every, passed = gathered(after(grads, next_a, prev_b))
    gate_grad, up_grad = weight_grads(inputs, gate_part, up_part)
    (down_grad,) = call(down_kernel, [((hidden, width), BF16)], [], act_rel, *every)
    returned, gate_grad, up_grad, down_grad = lax.optimization_barrier(
        (returned, gate_grad, up_grad, down_grad)
    )

    core = lax.rem(lax.axis_index("sp"), 2)
    side = share // 2
    mid_grad, sent, kept = call(
        return_kernel,
        [
            ((tok_rows, share), BF16),
            ((groups, side, hidden), BF16),
            ((groups, side, hidden), F32),
        ],
        [pltpu.VMEM((experts * packed, 128), F32)],
        core[None],
        routes.T,
        returned.reshape(experts * packed, 128),
        own_cols,
        gated_all,
    )
    swapped = lax.ppermute(sent, "sp", [(i, i ^ 1) for i in range(sources)])

    mid_left = turn(mid_grad, 1)
    mid_right = turn(mid_grad, -1)
    mid_far = turn(mid_grad, 2)

    paired = (kept + swapped.astype(F32)).astype(BF16)
    chips = sources // 2
    owned = width // sources
    pieces = lax.all_to_all(
        paired.reshape(chips, owned, hidden),
        "sp",
        0,
        0,
        axis_index_groups=[[2 * j + c for j in range(chips)] for c in range(2)],
        tiled=True,
    )
    out_weight_sum = jnp.sum(pieces.astype(F32), axis=0)
    per = chips // groups
    pairs = []
    for j in range(chips):
        for c in range(2):
            for m in range(groups):
                s = (sources // groups) * m + per * c + j % per
                pairs.append(((2 * j + c) * groups + m, s * groups + (m + j // per) % groups))
    out_weight_grad = lax.ppermute(out_weight_sum, ("sp", "tp"), pairs)

    mid_rel = jnp.concatenate([mid_grad, mid_right, mid_far, mid_left], axis=1)
    gated_grad = mm(mid_rel, out_weight_rel, ((1,), (0,)))
    out_gate_grad = (gated_grad * conv).astype(BF16)
    conv_grad = gated_grad * out_gate.astype(F32)
    later = passed_along(conv_grad[:reach], "sp", -1)
    following = jnp.concatenate([conv_grad, later], axis=0)
    mixed_grad = jnp.zeros_like(conv_grad)
    for tap in range(reach + 1):
        mixed_grad = mixed_grad + taps[tap][None, :] * following[tap : tap + tok_rows]
    input_grad = (mixed_grad * in_gate.astype(F32)).astype(BF16)
    in_gate_grad = (mixed_grad * conv_input.astype(F32)).astype(BF16)
    return (
        gate_grad[None],
        up_grad[None],
        down_grad[None],
        mid_grad,
        out_weight_grad,
        input_grad,
        out_gate_grad,
        in_gate_grad,
    )


def solution(mesh):
    in_specs = (
        P("sp", None),
        P("sp", None),
        P("sp", None),
        P(None, "sp", None, None),
        P("sp", None, "tp"),
        P("sp", None, "tp"),
        P("sp", "tp", None),
        P("sp", "tp"),
        P("sp", "tp"),
        P("sp", "tp"),
        P(None, "tp"),
        P(None, "tp"),
    )
    out_specs = (
        P("sp", None, "tp"),
        P("sp", None, "tp"),
        P("sp", "tp", None),
        P("sp", "tp"),
        P("sp", "tp"),
        P("sp", "tp"),
        P("sp", "tp"),
        P("sp", "tp"),
    )

    return jax.shard_map(
        on_device, mesh=mesh, in_specs=in_specs, out_specs=out_specs, check_vma=False
    )
```

profile of v0, /device:TPU:15, one launch (start us, length us, event | category | flops | bytes accessed | tf_op | source)
XLA Modules:
  0.0 199.3 jit_solution(16314556520339933721)
XLA Ops:
  0.9 1.3 collective-permute-start.1
  2.2 1.1 copy-done.9
  4.7 1.9 shard_map.179
  6.7 13.1 %all-to-all-start = ((bf16[64,48,128]{2,1,0:T(8,128)(2,1)}), bf16[64,48,128]{2,1,0:T(8,128)(2,1)S(1)}, u32[]{:S(2)}, u32[]{:S(2)}) async-start(bf16[64,48,128]{2,1,0:T(8,128)(2,1)} %bitcast.4), calls=%async_computation | async-start | bytes 1572864 | tf_op jit(solution)/shard_map/all_to_all | solution.py:293
  19.8 5.3 %collective-permute-done.w1_hbm = bf16[256,2048]{1,0:T(8,128)(2,1)S(1)} collective-permute-done((bf16[256,2048]{1,0:T(8,128)(2,1)}, bf16[256,2048]{1,0:T(8,128)(2,1)S(1)}, u32[]{:S(2)}, u32[]{:S(2)}) %collective-permute-start) | collective-permute-done | bytes 1048608 | tf_op jit(solution)/shard_map/ppermute | solution.py:225
  26.0 1.3 collective-permute-start.6
  27.3 1.9 slice.56
  29.4 5.1 %collective-permute-start.2 = (f32[2,256]{1,0:T(2,128)S(1)}, f32[2,256]{1,0:T(2,128)S(1)}, u32[]{:S(2)}, u32[]{:S(2)}) collective-permute-start(f32[2,256]{1,0:T(2,128)S(1)} %slice.57), channel_id=1, source_target_pairs={{0,4},{4,8},{8,12},{12,16},{16,20},{20,24},{24,28},{28,32},{32,36}... | collective-permute-start | bytes 6152 | tf_op jit(solution)/shard_map/ppermute | solution.py:231
  34.5 3.0 %fusion = bf16[2048,256]{1,0:T(8,128)(2,1)} fusion(s32[]{:T(128)S(6)} %select_n.10, bf16[2048,256]{1,0:T(8,128)(2,1)} %param.23), kind=kLoop, calls=%fused_computation.2 | loop fusion | flops 2097152 | bytes 2097156 | tf_op jit(solution)/shard_map/concatenate | solution.py:310
  38.6 2.3 %multiply_convert_fusion = (bf16[768,256]{1,0:T(8,128)(2,1)S(1)}, f32[768,256]{1,0:T(8,128)}, f32[768,256]{1,0:T(8,128)}) fusion(f32[768,256]{1,0:T(8,128)S(1)} %fusion.27, bf16[768,2048]{1,0:T(8,128)(2,1)S(1)} %bitcast.45, bf16[1,2048,256]{2,1,0:T(8,128)(2,1)S(1)} %copy-done.1), kind=kOutput, calls=%fused_computation.17 | convolution fusion | flops 807469056 | bytes 6946816 | tf_op jit(solution)/shard_map/dot_general | solution.py:14
  41.9 2.6 %collective-permute-start.5 = (bf16[192,256]{1,0:T(8,128)(2,1)S(1)}, bf16[192,256]{1,0:T(8,128)(2,1)S(1)}, u32[]{:S(2)}, u32[]{:S(2)}) collective-permute-start(bf16[192,256]{1,0:T(8,128)(2,1)S(1)} %get-tuple-element.86), channel_id=1, source_target_pairs={{0,1},{1,2},{2,3},{3,0},{4,5},{5,6},{6,7},{7,4},{8,9},{9,10},{10,1... | collective-permute-start | bytes 294920 | tf_op jit(solution)/shard_map/ppermute | solution.py:225
  46.1 2.5 %collective-permute-done.5 = bf16[192,256]{1,0:T(8,128)(2,1)S(1)} collective-permute-done((bf16[192,256]{1,0:T(8,128)(2,1)S(1)}, bf16[192,256]{1,0:T(8,128)(2,1)S(1)}, u32[]{:S(2)}, u32[]{:S(2)}) %collective-permute-start.5) | collective-permute-done | bytes 98336 | tf_op jit(solution)/shard_map/ppermute | solution.py:225
  48.5 2.1 %collective-permute-done.4 = bf16[192,256]{1,0:T(8,128)(2,1)S(1)} collective-permute-done((bf16[192,256]{1,0:T(8,128)(2,1)S(1)}, bf16[192,256]{1,0:T(8,128)(2,1)S(1)}, u32[]{:S(2)}, u32[]{:S(2)}) %collective-permute-start.4) | collective-permute-done | bytes 98336 | tf_op jit(solution)/shard_map/ppermute | solution.py:225
  50.6 1.3 collective-permute-done.3
  52.8 1.2 copy-done.5
  54.0 1.2 copy-done.10
  55.2 4.5 %shard_map.180 = (bf16[192,2048]{1,0:T(8,128)(2,1)}, bf16[192,256]{1,0:T(8,128)(2,1)S(1)}, bf16[192,256]{1,0:T(8,128)(2,1)S(1)}, bf16[192,256]{1,0:T(8,128)(2,1)S(1)}, bf16[192,256]{1,0:T(8,128)(2,1)S(1)}) custom-call(bf16[3072,128]{1,0:T(8,128)(2,1)S(1)} %bitcast.42, bf16[256,2048]{1,0:T(8,128)(2,1)S(1)} %bitcast.49, bf16[256,2048]{1,0:T(8,128)(2,1)S(1)} %copy-done.5, ...), custom_call_target="tpu_custom_call" | custom-call | tf_op jit(solution)/shard_map/pallas_call | solution.py:213
  59.8 1.8 collective-permute-start.9
  62.4 4.8 %collective-permute-done.8.right = bf16[192,256]{1,0:T(8,128)(2,1)S(1)} collective-permute-done((bf16[192,256]{1,0:T(8,128)(2,1)S(1)}, bf16[192,256]{1,0:T(8,128)(2,1)S(1)}, u32[]{:S(2)}, u32[]{:S(2)}) %collective-permute-start.8) | collective-permute-done | bytes 98336 | tf_op jit(solution)/shard_map/ppermute | solution.py:225
  68.2 2.7 %collective-permute-start.11 = (bf16[384,512]{1,0:T(8,128)(2,1)S(1)}, bf16[384,512]{1,0:T(8,128)(2,1)S(1)}, u32[]{:S(2)}, u32[]{:S(2)}) collective-permute-start(bf16[384,512]{1,0:T(8,128)(2,1)S(1)} %get-tuple-element.63), channel_id=1, source_target_pairs={{0,1},{1,2},{2,3},{3,0},{4,5},{5,6},{6,7},{7,4},{8,9},{9,10},{10,1... | collective-permute-start | bytes 1179656 | tf_op jit(solution)/shard_map/ppermute | solution.py:225
  70.9 1.4 shard_map.182
  72.5 2.8 %collective-permute-start.14 = (bf16[384,512]{1,0:T(8,128)(2,1)S(1)}, bf16[384,512]{1,0:T(8,128)(2,1)S(1)}, u32[]{:S(2)}, u32[]{:S(2)}) collective-permute-start(bf16[384,512]{1,0:T(8,128)(2,1)S(1)} %get-tuple-element.65), channel_id=1, source_target_pairs={{0,1},{1,2},{2,3},{3,0},{4,5},{5,6},{6,7},{7,4},{8,9},{9,10},{10,1... | collective-permute-start | bytes 1179656 | tf_op jit(solution)/shard_map/ppermute | solution.py:225
  75.2 3.4 %collective-permute-done.11 = bf16[384,512]{1,0:T(8,128)(2,1)S(1)} collective-permute-done((bf16[384,512]{1,0:T(8,128)(2,1)S(1)}, bf16[384,512]{1,0:T(8,128)(2,1)S(1)}, u32[]{:S(2)}, u32[]{:S(2)}) %collective-permute-start.11) | collective-permute-done | bytes 393248 | tf_op jit(solution)/shard_map/ppermute | solution.py:225
  78.7 3.5 %collective-permute-start.12 = (bf16[384,512]{1,0:T(8,128)(2,1)S(1)}, bf16[384,512]{1,0:T(8,128)(2,1)S(1)}, u32[]{:S(2)}, u32[]{:S(2)}) collective-permute-start(bf16[384,512]{1,0:T(8,128)(2,1)S(1)} %add_convert_fusion.2), channel_id=1, source_target_pairs={{0,1},{1,2},{2,3},{3,0},{4,5},{5,6},{6,7},{7,4},{8,9},{9,10},{10,1... | collective-permute-start | bytes 1179656 | tf_op jit(solution)/shard_map/ppermute | solution.py:225
  82.4 7.8 %collective-permute-done.13.right_a = bf16[384,512]{1,0:T(8,128)(2,1)S(1)} collective-permute-done((bf16[384,512]{1,0:T(8,128)(2,1)S(1)}, bf16[384,512]{1,0:T(8,128)(2,1)S(1)}, u32[]{:S(2)}, u32[]{:S(2)}) %collective-permute-start.13) | collective-permute-done | bytes 393248 | tf_op jit(solution)/shard_map/ppermute | solution.py:225
  90.2 5.3 %collective-permute-done.12.left_a = bf16[384,512]{1,0:T(8,128)(2,1)S(1)} collective-permute-done((bf16[384,512]{1,0:T(8,128)(2,1)S(1)}, bf16[384,512]{1,0:T(8,128)(2,1)S(1)}, u32[]{:S(2)}, u32[]{:S(2)}) %collective-permute-start.12) | collective-permute-done | bytes 393248 | tf_op jit(solution)/shard_map/ppermute | solution.py:225
  95.5 3.1 %collective-permute-done.16.right_b = bf16[384,512]{1,0:T(8,128)(2,1)S(1)} collective-permute-done((bf16[384,512]{1,0:T(8,128)(2,1)S(1)}, bf16[384,512]{1,0:T(8,128)(2,1)S(1)}, u32[]{:S(2)}, u32[]{:S(2)}) %collective-permute-start.16) | collective-permute-done | bytes 393248 | tf_op jit(solution)/shard_map/ppermute | solution.py:225
  98.6 1.5 shard_map.183
  100.1 13.8 %all-to-all-start.1 = ((bf16[64,48,128]{2,1,0:T(8,128)(2,1)}), bf16[64,48,128]{2,1,0:T(8,128)(2,1)S(1)}, u32[]{:S(2)}, u32[]{:S(2)}) async-start(bf16[64,48,128]{2,1,0:T(8,128)(2,1)} %bitcast.20), calls=%async_computation.1 | async-start | bytes 1572864 | tf_op jit(solution)/shard_map/all_to_all | solution.py:391
  114.2 1.5 collective-permute-start.18
  115.7 17.4 %collective-permute-done.17.g1 = bf16[192,2048]{1,0:T(8,128)(2,1)S(1)} collective-permute-done((bf16[192,2048]{1,0:T(8,128)(2,1)}, bf16[192,2048]{1,0:T(8,128)(2,1)S(1)}, u32[]{:S(2)}, u32[]{:S(2)}) %collective-permute-start.17) | collective-permute-done | bytes 786464 | tf_op jit(solution)/shard_map/ppermute | solution.py:225
  133.9 1.2 collective-permute-start.19
  136.2 1.9 copy-done.3
  139.1 3.6 %weights.1 = (bf16[2048,256]{1,0:T(8,128)(2,1)}, bf16[2048,256]{1,0:T(8,128)(2,1)}) custom-call(bf16[768,2048]{1,0:T(8,128)(2,1)S(1)} %bitcast.46, bf16[768,256]{1,0:T(8,128)(2,1)S(1)} %get-tuple-element.59.gate_part, bf16[768,256]{1,0:T(8,128)(2,1)S(1)} %copy-done.8), custom_call_target="tpu_custom_call" | custom-call | tf_op jit(solution)/shard_map/weights/pallas_call | solution.py:198
  143.7 2.9 %collective-permute-done.20.g3b = bf16[96,2048]{1,0:T(8,128)(2,1)} collective-permute-done((bf16[96,2048]{1,0:T(8,128)(2,1)}, bf16[96,2048]{1,0:T(8,128)(2,1)}, u32[]{:S(2)}, u32[]{:S(2)}) %collective-permute-start.20) | collective-permute-done | bytes 393248 | tf_op jit(solution)/shard_map/ppermute | solution.py:225
  146.6 3.9 %shard_map.184 = bf16[256,2048]{1,0:T(8,128)(2,1)} custom-call(bf16[4,192,256]{2,1,0:T(8,128)(2,1)S(1)} %fusion.10.act, bf16[192,2048]{1,0:T(8,128)(2,1)} %get-tuple-element.72.g0, bf16[192,2048]{1,0:T(8,128)(2,1)S(1)} %collective-permute-done.17.g1, bf16[192,2048]{1,0:T(8,128)(2,1)S(1)} %collective-permute-done.18.g2, ...), custom_call_target="tpu_custom_call" | custom-call | tf_op jit(solution)/shard_map/pallas_call | solution.py:213
  150.5 1.6 shard_map.185
  152.1 2.4 %collective-permute-start.21 = (bf16[4,256,256]{2,1,0:T(8,128)(2,1)S(1)}, bf16[4,256,256]{2,1,0:T(8,128)(2,1)S(1)}, u32[]{:S(2)}, u32[]{:S(2)}) collective-permute-start(bf16[4,256,256]{2,1,0:T(8,128)(2,1)S(1)} %get-tuple-element.81), channel_id=1, source_target_pairs={{0,4},{4,0},{8,12},{12,8},{16,20},{20,16},{24,28},{28,24},{32,36},... | collective-permute-start | bytes 1572872 | tf_op jit(solution)/shard_map/ppermute | solution.py:418
  154.5 1.5 collective-permute-done.21
  157.0 9.3 %all-to-all-start.2 = ((bf16[32,32,256]{2,1,0:T(8,128)(2,1)}), bf16[32,32,256]{2,1,0:T(8,128)(2,1)S(1)}, u32[]{:S(2)}, u32[]{:S(2)}) async-start(bf16[32,32,256]{2,1,0:T(8,128)(2,1)} %bitcast.26), calls=%async_computation.2 | async-start | bytes 1048576 | tf_op jit(solution)/shard_map/all_to_all | solution.py:427
  167.9 4.1 %collective-permute-done.25 = bf16[192,512]{1,0:T(8,128)(2,1)S(1)} collective-permute-done((bf16[192,512]{1,0:T(8,128)(2,1)S(1)}, bf16[192,512]{1,0:T(8,128)(2,1)S(1)}, u32[]{:S(2)}, u32[]{:S(2)}) %collective-permute-start.25) | collective-permute-done | bytes 196640 | tf_op jit(solution)/shard_map/ppermute | solution.py:225
  172.0 1.6 collective-permute-done.24
  173.6 5.5 %collective-permute-done.23 = bf16[192,512]{1,0:T(8,128)(2,1)S(1)} collective-permute-done((bf16[192,512]{1,0:T(8,128)(2,1)S(1)}, bf16[192,512]{1,0:T(8,128)(2,1)S(1)}, u32[]{:S(2)}, u32[]{:S(2)}) %collective-permute-start.23) | collective-permute-done | bytes 196640 | tf_op jit(solution)/shard_map/ppermute | solution.py:225
  179.1 1.0 multiply_convert_fusion.1
  180.1 2.4 %collective-permute-start.26 = (f32[2,256]{1,0:T(2,128)S(1)}, f32[2,256]{1,0:T(2,128)S(1)}, u32[]{:S(2)}, u32[]{:S(2)}) collective-permute-start(f32[2,256]{1,0:T(2,128)S(1)} %slice.62), channel_id=1, source_target_pairs={{4,0},{8,4},{12,8},{16,12},{20,16},{24,20},{28,24},{32,28},{36,32}... | collective-permute-start | bytes 6152 | tf_op jit(solution)/shard_map/ppermute | solution.py:231
  182.5 2.5 %collective-permute-done.26 = f32[2,256]{1,0:T(2,128)S(1)} collective-permute-done((f32[2,256]{1,0:T(2,128)S(1)}, f32[2,256]{1,0:T(2,128)S(1)}, u32[]{:S(2)}, u32[]{:S(2)}) %collective-permute-start.26) | collective-permute-done | bytes 2080 | tf_op jit(solution)/shard_map/ppermute | solution.py:231
  185.8 4.4 %collective-permute-start.22 = (f32[32,256]{1,0:T(8,128)S(1)}, f32[32,256]{1,0:T(8,128)S(1)}, u32[]{:S(2)}, u32[]{:S(2)}) collective-permute-start(f32[32,256]{1,0:T(8,128)S(1)} %convert_reduce_fusion), channel_id=1, source_target_pairs={{0,0},{1,65},{2,130},{3,195},{4,32},{5,97},{6,162},{7,227},{8,4},{... | collective-permute-start | bytes 98312 | tf_op jit(solution)/shard_map/ppermute | solution.py:443
  190.9 7.8 %collective-permute-done.22 = f32[32,256]{1,0:T(8,128)S(1)} collective-permute-done((f32[32,256]{1,0:T(8,128)S(1)}, f32[32,256]{1,0:T(8,128)S(1)}, u32[]{:S(2)}, u32[]{:S(2)}) %collective-permute-start.22) | collective-permute-done | bytes 32800 | tf_op jit(solution)/shard_map/ppermute | solution.py:443
  (95 shorter events, 18.1 us)
Async XLA Ops:
  0.6 19.1 %copy-start.24 = (f32[3,256]{1,0:T(4,128)S(1)}, f32[3,256]{1,0:T(4,128)}, u32[]{:S(2)}) copy-start(f32[3,256]{1,0:T(4,128)} %param.22) | copy-start | bytes 9220
  0.6 24.4 %collective-permute-start = (bf16[256,2048]{1,0:T(8,128)(2,1)}, bf16[256,2048]{1,0:T(8,128)(2,1)S(1)}, u32[]{:S(2)}, u32[]{:S(2)}) collective-permute-start(bf16[256,2048]{1,0:T(8,128)(2,1)} %bitcast.47), channel_id=1, source_target_pairs={{0,1},{1,2},{2,3},{3,0},{4,5},{5,6},{6,7},{7,4},{8,9},{9,10},{10,1... | collective-permute-start | bytes 3145736 | tf_op jit(solution)/shard_map/ppermute | solution.py:225
  0.9 26.4 %collective-permute-start.1 = (bf16[256,2048]{1,0:T(8,128)(2,1)}, bf16[256,2048]{1,0:T(8,128)(2,1)}, u32[]{:S(2)}, u32[]{:S(2)}) collective-permute-start(bf16[256,2048]{1,0:T(8,128)(2,1)} %bitcast.48), channel_id=1, source_target_pairs={{0,3},{1,0},{2,1},{3,2},{4,7},{5,4},{6,5},{7,6},{8,11},{9,8},{10,9... | collective-permute-start | bytes 3145736 | tf_op jit(solution)/shard_map/ppermute | solution.py:225
  6.6 22.7 %copy-start.17 = (bf16[192,256]{1,0:T(8,128)(2,1)S(1)}, bf16[192,256]{1,0:T(8,128)(2,1)}, u32[]{:S(2)}) copy-start(bf16[192,256]{1,0:T(8,128)(2,1)} %param.19) | copy-start | bytes 294916
  6.6 22.7 %copy-start.19 = (bf16[192,256]{1,0:T(8,128)(2,1)S(1)}, bf16[192,256]{1,0:T(8,128)(2,1)}, u32[]{:S(2)}) copy-start(bf16[192,256]{1,0:T(8,128)(2,1)} %param.21) | copy-start | bytes 294916
  6.7 46.1 %all-to-all-start = ((bf16[64,48,128]{2,1,0:T(8,128)(2,1)}), bf16[64,48,128]{2,1,0:T(8,128)(2,1)S(1)}, u32[]{:S(2)}, u32[]{:S(2)}) async-start(bf16[64,48,128]{2,1,0:T(8,128)(2,1)} %bitcast.4), calls=%async_computation | async-start | bytes 1572864 | tf_op jit(solution)/shard_map/all_to_all | solution.py:293
  19.8 17.6 %copy-start = (bf16[1,2048,256]{2,1,0:T(8,128)(2,1)S(1)}, bf16[1,2048,256]{2,1,0:T(8,128)(2,1)}, u32[]{:S(2)}) copy-start(bf16[1,2048,256]{2,1,0:T(8,128)(2,1)} %param.16) | copy-start | bytes 3145732
  19.8 17.6 %copy-start.2 = (bf16[64,1,12,2048]{3,0,2,1:T(8,128)(2,1)S(1)}, bf16[64,1,12,2048]{3,0,2,1:T(8,128)(2,1)}, u32[]{:S(2)}) copy-start(bf16[64,1,12,2048]{3,0,2,1:T(8,128)(2,1)} %param.15) | copy-start | bytes 9437188
  25.1 12.3 %copy-start.4 = (bf16[256,2048]{1,0:T(8,128)(2,1)}, bf16[256,2048]{1,0:T(8,128)(2,1)S(1)}, u32[]{:S(2)}) copy-start(bf16[256,2048]{1,0:T(8,128)(2,1)S(1)} %collective-permute-done.w1_hbm) | copy-start | bytes 3145732
  26.0 26.8 %collective-permute-start.6 = (bf16[128,2048]{1,0:T(8,128)(2,1)}, bf16[128,2048]{1,0:T(8,128)(2,1)}, u32[]{:S(2)}, u32[]{:S(2)}) collective-permute-start(bf16[128,2048]{1,0:T(8,128)(2,1)} %slice.55), channel_id=1, source_target_pairs={{0,1},{1,2},{2,3},{3,0},{4,5},{5,6},{6,7},{7,4},{8,9},{9,10},{10,1... | collective-permute-start | bytes 1572872 | tf_op jit(solution)/shard_map/ppermute | solution.py:225
  29.2 23.6 %collective-permute-start.7 = (bf16[128,2048]{1,0:T(8,128)(2,1)}, bf16[128,2048]{1,0:T(8,128)(2,1)}, u32[]{:S(2)}, u32[]{:S(2)}) collective-permute-start(bf16[128,2048]{1,0:T(8,128)(2,1)} %slice.56), channel_id=1, source_target_pairs={{0,3},{1,0},{2,1},{3,2},{4,7},{5,4},{6,5},{7,6},{8,11},{9,8},{10,9... | collective-permute-start | bytes 1572872 | tf_op jit(solution)/shard_map/ppermute | solution.py:225
  29.4 11.7 %collective-permute-start.2 = (f32[2,256]{1,0:T(2,128)S(1)}, f32[2,256]{1,0:T(2,128)S(1)}, u32[]{:S(2)}, u32[]{:S(2)}) collective-permute-start(f32[2,256]{1,0:T(2,128)S(1)} %slice.57), channel_id=1, source_target_pairs={{0,4},{4,8},{8,12},{12,16},{16,20},{20,24},{24,28},{28,32},{32,36}... | collective-permute-start | bytes 6152 | tf_op jit(solution)/shard_map/ppermute | solution.py:231
  38.6 2.5 %copy-start.22 = (bf16[192,256]{1,0:T(8,128)(2,1)S(1)}, bf16[192,256]{1,0:T(8,128)(2,1)}, u32[]{:S(2)}) copy-start(bf16[192,256]{1,0:T(8,128)(2,1)} %param.20) | copy-start | bytes 294916
  41.9 6.6 %collective-permute-start.5 = (bf16[192,256]{1,0:T(8,128)(2,1)S(1)}, bf16[192,256]{1,0:T(8,128)(2,1)S(1)}, u32[]{:S(2)}, u32[]{:S(2)}) collective-permute-start(bf16[192,256]{1,0:T(8,128)(2,1)S(1)} %get-tuple-element.86), channel_id=1, source_target_pairs={{0,1},{1,2},{2,3},{3,0},{4,5},{5,6},{6,7},{7,4},{8,9},{9,10},{10,1... | collective-permute-start | bytes 294920 | tf_op jit(solution)/shard_map/ppermute | solution.py:225
  44.5 6.1 %collective-permute-start.4 = (bf16[192,256]{1,0:T(8,128)(2,1)S(1)}, bf16[192,256]{1,0:T(8,128)(2,1)S(1)}, u32[]{:S(2)}, u32[]{:S(2)}) collective-permute-start(bf16[192,256]{1,0:T(8,128)(2,1)S(1)} %get-tuple-element.86), channel_id=1, source_target_pairs={{0,2},{1,3},{2,0},{3,1},{4,6},{5,7},{6,4},{7,5},{8,10},{9,11},{10,... | collective-permute-start | bytes 294920 | tf_op jit(solution)/shard_map/ppermute | solution.py:225
  44.5 7.4 %collective-permute-start.3 = (bf16[192,256]{1,0:T(8,128)(2,1)S(1)}, bf16[192,256]{1,0:T(8,128)(2,1)S(1)}, u32[]{:S(2)}, u32[]{:S(2)}) collective-permute-start(bf16[192,256]{1,0:T(8,128)(2,1)S(1)} %get-tuple-element.86), channel_id=1, source_target_pairs={{0,3},{1,0},{2,1},{3,2},{4,7},{5,4},{6,5},{7,6},{8,11},{9,8},{10,9... | collective-permute-start | bytes 294920 | tf_op jit(solution)/shard_map/ppermute | solution.py:225
  55.2 12.3 %copy-start.11 = (f32[768,256]{1,0:T(8,128)S(1)}, f32[768,256]{1,0:T(8,128)}, u32[]{:S(2)}) copy-start(f32[768,256]{1,0:T(8,128)} %get-tuple-element.58.gate_of) | copy-start | bytes 2359300
  55.2 12.3 %copy-start.12 = (f32[768,256]{1,0:T(8,128)S(1)}, f32[768,256]{1,0:T(8,128)}, u32[]{:S(2)}) copy-start(f32[768,256]{1,0:T(8,128)} %get-tuple-element.57.up_of) | copy-start | bytes 2359300
  59.7 7.6 %collective-permute-start.8 = (bf16[192,256]{1,0:T(8,128)(2,1)S(1)}, bf16[192,256]{1,0:T(8,128)(2,1)S(1)}, u32[]{:S(2)}, u32[]{:S(2)}) collective-permute-start(bf16[192,256]{1,0:T(8,128)(2,1)S(1)} %get-tuple-element.54), channel_id=1, source_target_pairs={{0,3},{1,0},{2,1},{3,2},{4,7},{5,4},{6,5},{7,6},{8,11},{9,8},{10,9... | collective-permute-start | bytes 294920 | tf_op jit(solution)/shard_map/ppermute | solution.py:225
  59.8 7.5 %collective-permute-start.9 = (bf16[192,256]{1,0:T(8,128)(2,1)S(1)}, bf16[192,256]{1,0:T(8,128)(2,1)S(1)}, u32[]{:S(2)}, u32[]{:S(2)}) collective-permute-start(bf16[192,256]{1,0:T(8,128)(2,1)S(1)} %get-tuple-element.55), channel_id=1, source_target_pairs={{0,2},{1,3},{2,0},{3,1},{4,6},{5,7},{6,4},{7,5},{8,10},{9,11},{10,... | collective-permute-start | bytes 294920 | tf_op jit(solution)/shard_map/ppermute | solution.py:225
  61.6 6.0 %collective-permute-start.10 = (bf16[192,256]{1,0:T(8,128)(2,1)S(1)}, bf16[192,256]{1,0:T(8,128)(2,1)S(1)}, u32[]{:S(2)}, u32[]{:S(2)}) collective-permute-start(bf16[192,256]{1,0:T(8,128)(2,1)S(1)} %get-tuple-element.56), channel_id=1, source_target_pairs={{0,1},{1,2},{2,3},{3,0},{4,5},{5,6},{6,7},{7,4},{8,9},{9,10},{10,1... | collective-permute-start | bytes 294920 | tf_op jit(solution)/shard_map/ppermute | solution.py:225
  68.2 14.1 %copy-start.7 = (bf16[768,256]{1,0:T(8,128)(2,1)}, bf16[768,256]{1,0:T(8,128)(2,1)S(1)}, u32[]{:S(2)}) copy-start(bf16[768,256]{1,0:T(8,128)(2,1)S(1)} %get-tuple-element.60.up_part) | copy-start | bytes 1179652
  68.2 10.4 %collective-permute-start.11 = (bf16[384,512]{1,0:T(8,128)(2,1)S(1)}, bf16[384,512]{1,0:T(8,128)(2,1)S(1)}, u32[]{:S(2)}, u32[]{:S(2)}) collective-permute-start(bf16[384,512]{1,0:T(8,128)(2,1)S(1)} %get-tuple-element.63), channel_id=1, source_target_pairs={{0,1},{1,2},{2,3},{3,0},{4,5},{5,6},{6,7},{7,4},{8,9},{9,10},{10,1... | collective-permute-start | bytes 1179656 | tf_op jit(solution)/shard_map/ppermute | solution.py:225
  70.9 11.3 %collective-permute-start.15 = (bf16[384,512]{1,0:T(8,128)(2,1)S(1)}, bf16[384,512]{1,0:T(8,128)(2,1)S(1)}, u32[]{:S(2)}, u32[]{:S(2)}) collective-permute-start(bf16[384,512]{1,0:T(8,128)(2,1)S(1)} %get-tuple-element.67), channel_id=1, source_target_pairs={{0,3},{1,0},{2,1},{3,2},{4,7},{5,4},{6,5},{7,6},{8,11},{9,8},{10,9... | collective-permute-start | bytes 1179656 | tf_op jit(solution)/shard_map/ppermute | solution.py:225
  72.4 17.8 %collective-permute-start.13 = (bf16[384,512]{1,0:T(8,128)(2,1)S(1)}, bf16[384,512]{1,0:T(8,128)(2,1)S(1)}, u32[]{:S(2)}, u32[]{:S(2)}) collective-permute-start(bf16[384,512]{1,0:T(8,128)(2,1)S(1)} %get-tuple-element.64), channel_id=1, source_target_pairs={{0,3},{1,0},{2,1},{3,2},{4,7},{5,4},{6,5},{7,6},{8,11},{9,8},{10,9... | collective-permute-start | bytes 1179656 | tf_op jit(solution)/shard_map/ppermute | solution.py:225
  72.5 17.7 %collective-permute-start.14 = (bf16[384,512]{1,0:T(8,128)(2,1)S(1)}, bf16[384,512]{1,0:T(8,128)(2,1)S(1)}, u32[]{:S(2)}, u32[]{:S(2)}) collective-permute-start(bf16[384,512]{1,0:T(8,128)(2,1)S(1)} %get-tuple-element.65), channel_id=1, source_target_pairs={{0,1},{1,2},{2,3},{3,0},{4,5},{5,6},{6,7},{7,4},{8,9},{9,10},{10,1... | collective-permute-start | bytes 1179656 | tf_op jit(solution)/shard_map/ppermute | solution.py:225
  78.7 16.8 %collective-permute-start.12 = (bf16[384,512]{1,0:T(8,128)(2,1)S(1)}, bf16[384,512]{1,0:T(8,128)(2,1)S(1)}, u32[]{:S(2)}, u32[]{:S(2)}) collective-permute-start(bf16[384,512]{1,0:T(8,128)(2,1)S(1)} %add_convert_fusion.2), channel_id=1, source_target_pairs={{0,1},{1,2},{2,3},{3,0},{4,5},{5,6},{6,7},{7,4},{8,9},{9,10},{10,1... | collective-permute-start | bytes 1179656 | tf_op jit(solution)/shard_map/ppermute | solution.py:225
  82.3 16.3 %collective-permute-start.16 = (bf16[384,512]{1,0:T(8,128)(2,1)S(1)}, bf16[384,512]{1,0:T(8,128)(2,1)S(1)}, u32[]{:S(2)}, u32[]{:S(2)}) collective-permute-start(bf16[384,512]{1,0:T(8,128)(2,1)S(1)} %add_convert_fusion.1), channel_id=1, source_target_pairs={{0,3},{1,0},{2,1},{3,2},{4,7},{5,4},{6,5},{7,6},{8,11},{9,8},{10,9... | collective-permute-start | bytes 1179656 | tf_op jit(solution)/shard_map/ppermute | solution.py:225
  100.1 50.3 %all-to-all-start.1 = ((bf16[64,48,128]{2,1,0:T(8,128)(2,1)}), bf16[64,48,128]{2,1,0:T(8,128)(2,1)S(1)}, u32[]{:S(2)}, u32[]{:S(2)}) async-start(bf16[64,48,128]{2,1,0:T(8,128)(2,1)} %bitcast.20), calls=%async_computation.1 | async-start | bytes 1572864 | tf_op jit(solution)/shard_map/all_to_all | solution.py:391
  113.9 19.2 %collective-permute-start.17 = (bf16[192,2048]{1,0:T(8,128)(2,1)}, bf16[192,2048]{1,0:T(8,128)(2,1)S(1)}, u32[]{:S(2)}, u32[]{:S(2)}) collective-permute-start(bf16[192,2048]{1,0:T(8,128)(2,1)} %get-tuple-element.72.g0), channel_id=1, source_target_pairs={{0,1},{1,2},{2,3},{3,0},{4,5},{5,6},{6,7},{7,4},{8,9},{9,10},{10,1... | collective-permute-start | bytes 2359304 | tf_op jit(solution)/shard_map/ppermute | solution.py:225
  114.2 20.9 %collective-permute-start.18 = (bf16[192,2048]{1,0:T(8,128)(2,1)}, bf16[192,2048]{1,0:T(8,128)(2,1)S(1)}, u32[]{:S(2)}, u32[]{:S(2)}) collective-permute-start(bf16[192,2048]{1,0:T(8,128)(2,1)} %get-tuple-element.72.g0), channel_id=1, source_target_pairs={{0,3},{1,0},{2,1},{3,2},{4,7},{5,4},{6,5},{7,6},{8,11},{9,8},{10,9... | collective-permute-start | bytes 2359304 | tf_op jit(solution)/shard_map/ppermute | solution.py:225
  133.9 9.7 %collective-permute-start.19 = (bf16[96,2048]{1,0:T(8,128)(2,1)}, bf16[96,2048]{1,0:T(8,128)(2,1)}, u32[]{:S(2)}, u32[]{:S(2)}) collective-permute-start(bf16[96,2048]{1,0:T(8,128)(2,1)} %slice.60), channel_id=1, source_target_pairs={{0,1},{1,2},{2,3},{3,0},{4,5},{5,6},{6,7},{7,4},{8,9},{9,10},{10,1... | collective-permute-start | bytes 1179656 | tf_op jit(solution)/shard_map/ppermute | solution.py:225
  135.9 10.7 %collective-permute-start.20 = (bf16[96,2048]{1,0:T(8,128)(2,1)}, bf16[96,2048]{1,0:T(8,128)(2,1)}, u32[]{:S(2)}, u32[]{:S(2)}) collective-permute-start(bf16[96,2048]{1,0:T(8,128)(2,1)} %slice.61), channel_id=1, source_target_pairs={{0,3},{1,0},{2,1},{3,2},{4,7},{5,4},{6,5},{7,6},{8,11},{9,8},{10,9... | collective-permute-start | bytes 1179656 | tf_op jit(solution)/shard_map/ppermute | solution.py:225
  142.7 7.8 %copy-start.6 = (bf16[4,192,256]{2,1,0:T(8,128)(2,1)S(1)}, bf16[4,192,256]{2,1,0:T(8,128)(2,1)}, u32[]{:S(2)}) copy-start(bf16[4,192,256]{2,1,0:T(8,128)(2,1)} %pad_maximum_fusion.gated_ref) | copy-start | bytes 1179652
  142.7 7.8 %copy-start.14 = (s32[192,2]{0,1:T(2,128)S(1)}, s32[192,2]{0,1:T(2,128)}, u32[]{:S(2)}) copy-start(s32[192,2]{0,1:T(2,128)} %param.13) | copy-start | bytes 4612
  152.1 26.9 %copy-start.16 = (bf16[2048,256]{1,0:T(8,128)(2,1)S(1)}, bf16[2048,256]{1,0:T(8,128)(2,1)}, u32[]{:S(2)}) copy-start(bf16[2048,256]{1,0:T(8,128)(2,1)} %fusion) | copy-start | bytes 3145732
  152.1 26.9 %copy-start.21 = (f32[192,256]{1,0:T(8,128)S(1)}, f32[192,256]{1,0:T(8,128)}, u32[]{:S(2)}) copy-start(f32[192,256]{1,0:T(8,128)} %get-tuple-element.83) | copy-start | bytes 589828
  152.1 27.0 %copy-start.23 = (bf16[192,256]{1,0:T(8,128)(2,1)S(1)}, bf16[192,256]{1,0:T(8,128)(2,1)}, u32[]{:S(2)}) copy-start(bf16[192,256]{1,0:T(8,128)(2,1)} %param.20) | copy-start | bytes 294916
  152.1 3.9 %collective-permute-start.21 = (bf16[4,256,256]{2,1,0:T(8,128)(2,1)S(1)}, bf16[4,256,256]{2,1,0:T(8,128)(2,1)S(1)}, u32[]{:S(2)}, u32[]{:S(2)}) collective-permute-start(bf16[4,256,256]{2,1,0:T(8,128)(2,1)S(1)} %get-tuple-element.81), channel_id=1, source_target_pairs={{0,4},{4,0},{8,12},{12,8},{16,20},{20,16},{24,28},{28,24},{32,36},... | collective-permute-start | bytes 1572872 | tf_op jit(solution)/shard_map/ppermute | solution.py:418
  156.1 10.3 %copy-start.25 = (bf16[192,512]{1,0:T(8,128)(2,1)S(1)}, bf16[192,512]{1,0:T(8,128)(2,1)}, u32[]{:S(2)}) copy-start(bf16[192,512]{1,0:T(8,128)(2,1)} %get-tuple-element.107) | copy-start | bytes 589828
  157.0 28.8 %all-to-all-start.2 = ((bf16[32,32,256]{2,1,0:T(8,128)(2,1)}), bf16[32,32,256]{2,1,0:T(8,128)(2,1)S(1)}, u32[]{:S(2)}, u32[]{:S(2)}) async-start(bf16[32,32,256]{2,1,0:T(8,128)(2,1)} %bitcast.26), calls=%async_computation.2 | async-start | bytes 1048576 | tf_op jit(solution)/shard_map/all_to_all | solution.py:427
  166.3 18.7 %copy-start.18 = (bf16[192,256]{1,0:T(8,128)(2,1)S(1)}, bf16[192,256]{1,0:T(8,128)(2,1)}, u32[]{:S(2)}) copy-start(bf16[192,256]{1,0:T(8,128)(2,1)} %param.19) | copy-start | bytes 294916
  166.3 23.9 %copy-start.20 = (bf16[192,256]{1,0:T(8,128)(2,1)S(1)}, bf16[192,256]{1,0:T(8,128)(2,1)}, u32[]{:S(2)}) copy-start(bf16[192,256]{1,0:T(8,128)(2,1)} %param.21) | copy-start | bytes 294916
  166.3 5.6 %collective-permute-start.25 = (bf16[192,512]{1,0:T(8,128)(2,1)S(1)}, bf16[192,512]{1,0:T(8,128)(2,1)S(1)}, u32[]{:S(2)}, u32[]{:S(2)}) collective-permute-start(bf16[192,512]{1,0:T(8,128)(2,1)S(1)} %copy-done.25), channel_id=1, source_target_pairs={{0,1},{1,2},{2,3},{3,0},{4,5},{5,6},{6,7},{7,4},{8,9},{9,10},{10,1... | collective-permute-start | bytes 589832 | tf_op jit(solution)/shard_map/ppermute | solution.py:225
  166.4 7.2 %collective-permute-start.24 = (bf16[192,512]{1,0:T(8,128)(2,1)S(1)}, bf16[192,512]{1,0:T(8,128)(2,1)S(1)}, u32[]{:S(2)}, u32[]{:S(2)}) collective-permute-start(bf16[192,512]{1,0:T(8,128)(2,1)S(1)} %copy-done.25), channel_id=1, source_target_pairs={{0,2},{1,3},{2,0},{3,1},{4,6},{5,7},{6,4},{7,5},{8,10},{9,11},{10,... | collective-permute-start | bytes 589832 | tf_op jit(solution)/shard_map/ppermute | solution.py:225
  167.3 11.8 %collective-permute-start.23 = (bf16[192,512]{1,0:T(8,128)(2,1)S(1)}, bf16[192,512]{1,0:T(8,128)(2,1)S(1)}, u32[]{:S(2)}, u32[]{:S(2)}) collective-permute-start(bf16[192,512]{1,0:T(8,128)(2,1)S(1)} %copy-done.25), channel_id=1, source_target_pairs={{0,3},{1,0},{2,1},{3,2},{4,7},{5,4},{6,5},{7,6},{8,11},{9,8},{10,9... | collective-permute-start | bytes 589832 | tf_op jit(solution)/shard_map/ppermute | solution.py:225
  180.1 4.9 %collective-permute-start.26 = (f32[2,256]{1,0:T(2,128)S(1)}, f32[2,256]{1,0:T(2,128)S(1)}, u32[]{:S(2)}, u32[]{:S(2)}) collective-permute-start(f32[2,256]{1,0:T(2,128)S(1)} %slice.62), channel_id=1, source_target_pairs={{4,0},{8,4},{12,8},{16,12},{20,16},{24,20},{28,24},{32,28},{36,32}... | collective-permute-start | bytes 6152 | tf_op jit(solution)/shard_map/ppermute | solution.py:231
  185.8 12.9 %collective-permute-start.22 = (f32[32,256]{1,0:T(8,128)S(1)}, f32[32,256]{1,0:T(8,128)S(1)}, u32[]{:S(2)}, u32[]{:S(2)}) collective-permute-start(f32[32,256]{1,0:T(8,128)S(1)} %convert_reduce_fusion), channel_id=1, source_target_pairs={{0,0},{1,65},{2,130},{3,195},{4,32},{5,97},{6,162},{7,227},{8,4},{... | collective-permute-start | bytes 98312 | tf_op jit(solution)/shard_map/ppermute | solution.py:443
  (8 other events, 9.1 us)
where the time goes:
time: 200 us; the launch traced here: 199 us
  waiting for transfers between devices  80.3 us (40%)
  starting transfers between devices  73.3 us (37%)
  Pallas kernels  19.1 us (10%)
  local copies, waits for them, and re-layouts  14 us (7%)
  other arithmetic  7.26 us (4%)
  matrix products  4.33 us (2%)
    ppermute x23, waiting for transfers between devices, turn(): lax.ppermute(shard, 'tp', [(i, (i + by) % peers) for i in range(peers)])  68.4 us
    ppermute x23, starting transfers between devices, turn(): lax.ppermute(shard, 'tp', [(i, (i + by) % peers) for i in range(peers)])  22.9 us
    pallas_call x7, Pallas kernels, call(): pl.pallas_call(kernel, out_shape=[jax.ShapeDtypeStruct(*o) for o in outs]...  15.5 us
    all_to_all x1, starting transfers between devices, on_device(): lax.all_to_all(leaving.reshape(sources, packed, 128), 'sp', split_axis=0,...  13.8 us
    all_to_all x1, starting transfers between devices, on_device(): lax.all_to_all(piece.reshape(experts, packed, 128), 'sp', split_axis=0, c...  13.1 us
    all_to_all x1, starting transfers between devices, on_device(): lax.all_to_all(paired.reshape(chips, owned, hidden), 'sp', 0, 0, axis_ind...  9.34 us
    unnamed x53, local copies, waits for them, and re-layouts  8.74 us
    ppermute x1, waiting for transfers between devices, on_device(): out_weight_grad = lax.ppermute(out_weight_sum, ('sp', 'tp'), pairs)  7.82 us
  transfers between devices with their start and end apart: 30, of which 19 were waited for; matrix products, arithmetic and copies ran while one was open for 8% of the time, Pallas kernels for 5%

commit v1 on v0

--- a/solution.py
+++ b/solution.py
@@ -58,17 +58,14 @@
 
 
 def arrive_kernel(
-    arrived_hbm, w0_hbm, w1_hbm, w2_hbm, w3a_hbm, w3b_hbm,
-    rows_ref, p0, p1, p2, p3, wide_ref, arrived_ref, w0, w1, w2, w3, sems,
+    arrived_hbm, w0_hbm, w1_hbm, w2_hbm,
+    rows_ref, p0, p1, p2, wide_ref, arrived_ref, w0, w1, w2, sems,
 ):
-    half = w3a_hbm.shape[0]
     loads = [
         pltpu.make_async_copy(arrived_hbm, arrived_ref, sems.at[0]),
-        pltpu.make_async_copy(w3a_hbm, w3.at[pl.ds(0, half), :], sems.at[1]),
-        pltpu.make_async_copy(w3b_hbm, w3.at[pl.ds(half, half), :], sems.at[2]),
-        pltpu.make_async_copy(w2_hbm, w2, sems.at[3]),
-        pltpu.make_async_copy(w1_hbm, w1, sems.at[4]),
-        pltpu.make_async_copy(w0_hbm, w0, sems.at[5]),
+        pltpu.make_async_copy(w2_hbm, w2, sems.at[1]),
+        pltpu.make_async_copy(w1_hbm, w1, sems.at[2]),
+        pltpu.make_async_copy(w0_hbm, w0, sems.at[3]),
     ]
     for load in loads:
         load.start()
@@ -82,12 +79,15 @@
             rows_ref[i * sources : (i + 1) * sources, g * 128 : (g + 1) * 128] = wide_ref[
                 pl.ds(i * lanes + g, sources, stride=per), :
             ].astype(BF16)
-    loads[1].wait()
-    loads[2].wait()
-    p3[...] = mm(rows_ref[...], w3[...], ((1,), (1,))).astype(BF16)
-    for load, w, p in ((loads[3], w2, p2), (loads[4], w1, p1), (loads[5], w0, p0)):
+    for load, w, p in ((loads[1], w2, p2), (loads[2], w1, p1), (loads[3], w0, p0)):
         load.wait()
         p[...] = mm(rows_ref[...], w[...], ((1,), (1,))).astype(BF16)
+
+
+def far_kernel(rows_ref, w3a, w3b, p3):
+    half = w3a.shape[0]
+    p3[:, :half] = mm(rows_ref[...], w3a[...], ((1,), (1,))).astype(BF16)
+    p3[:, half:] = mm(rows_ref[...], w3b[...], ((1,), (1,))).astype(BF16)
 
 
 def row_block(gate_part, up_part, gate_ref, up_ref, which, share):
@@ -150,22 +150,26 @@
 
 
 def return_kernel(
-    core_ref, routes_ref, returned_ref, own_ref, gated_ref,
-    mid_ref, sent_ref, kept_ref, wide_ref,
+    where_ref, routes_ref, returned_ref, tokens_hbm, gated_ref,
+    mid_ref, sent_ref, kept_ref, wide_ref, own_ref, sem,
 ):
     share = mid_ref.shape[1]
+    first = pl.multiple_of(where_ref[0] * share, share)
+    load = pltpu.make_async_copy(tokens_hbm.at[:, pl.ds(first, share)], own_ref, sem)
+    load.start()
     lanes = share // 128
     columns = returned_ref.shape[0] // lanes
     wide_ref[...] = returned_ref[...].astype(F32)
     _, named, place, slot = slot_hits(routes_ref, columns // 64, columns)
     hit = jnp.where(place == slot, named, 0.0).T.astype(BF16)
+    load.wait()
     for g in range(lanes):
         rows = wide_ref[pl.ds(g, columns, stride=lanes), :].astype(BF16)
         picked = mm(hit, rows, ((1,), (0,)))
         own = own_ref[:, g * 128 : (g + 1) * 128].astype(F32)
         mid_ref[:, g * 128 : (g + 1) * 128] = (own + picked).astype(BF16)
     side = share // 2
-    core = core_ref[0]
+    core = where_ref[1]
     for ref, which in ((sent_ref, 1 - core), (kept_ref, core)):
         columns_t = mid_ref[:, pl.ds(pl.multiple_of(which * side, side), side)].T
         for r in range(gated_ref.shape[0]):
@@ -173,14 +177,31 @@
             ref[r] = part.astype(ref.dtype)
 
 
-def down_kernel(act, g0, g1, g2, g3a, g3b, out_ref):
+def down_kernel(member_ref, act, g0, g1, g2, g3a, g3b, out_ref):
     half = g3a.shape[0]
-    total = mm(act[0].T, g0[...], ((1,), (0,)))
-    total = total + mm(act[3].T, g1[...], ((1,), (0,)))
-    total = total + mm(act[1].T, g2[...], ((1,), (0,)))
-    total = total + mm(act[2, :half].T, g3a[...], ((1,), (0,)))
-    total = total + mm(act[2, half:].T, g3b[...], ((1,), (0,)))
+
+    def block(by):
+        return act[lax.rem(member_ref[0] + by, 4)]
+
+    total = mm(block(0).T, g0[...], ((1,), (0,)))
+    total = total + mm(block(3).T, g1[...], ((1,), (0,)))
+    total = total + mm(block(1).T, g2[...], ((1,), (0,)))
+    far = block(2)
+    total = total + mm(far[:half].T, g3a[...], ((1,), (0,)))
+    total = total + mm(far[half:].T, g3b[...], ((1,), (0,)))
     out_ref[...] = total.astype(BF16)
+
+
+def halves_kernel(left, right, a, b, sems):
+    half = a.shape[0]
+    copies = [
+        pltpu.make_async_copy(left.at[pl.ds(0, half), :], a, sems.at[0]),
+        pltpu.make_async_copy(right.at[pl.ds(half, half), :], b, sems.at[1]),
+    ]
+    for copy in copies:
+        copy.start()
+    for copy in copies:
+        copy.wait()
 
 
 def weights_kernel(x_ref, gate_part, up_part, gate_ref, up_ref):
@@ -206,17 +227,17 @@
     )(inputs, gate_part, up_part)
 
 
-def call(kernel, outs, scratch, *args, there=False):
+def call(kernel, outs, scratch, *args, there=(), limit=40 << 20):
     smem = pl.BlockSpec(memory_space=pltpu.SMEM)
     vmem = pl.BlockSpec(memory_space=pltpu.VMEM)
-    hbm = pl.BlockSpec(memory_space=pl.ANY)
+    hbm = pl.BlockSpec(memory_space=pltpu.HBM)
     return pl.pallas_call(
         kernel,
         out_shape=[jax.ShapeDtypeStruct(*o) for o in outs],
-        in_specs=[smem if a.ndim == 1 else hbm if there else vmem for a in args],
+        in_specs=[smem if a.ndim == 1 else hbm if i in there else vmem for i, a in enumerate(args)],
         out_specs=[vmem] * len(outs),
         scratch_shapes=scratch,
-        compiler_params=pltpu.CompilerParams(vmem_limit_bytes=40 << 20),
+        compiler_params=pltpu.CompilerParams(vmem_limit_bytes=limit),
     )(*args)
 
 
@@ -235,15 +256,23 @@
     return lax.optimization_barrier((value, *others))[0]
 
 
-def gathered(own):
-    half = own.shape[0] // 2
+def gathered(own, *earlier):
     left = turn(own, 1)
     right = turn(own, -1)
-    passed_a = left[:half]
+    left, right, *earlier = lax.optimization_barrier((left, right, *earlier))
+    half = (own.shape[0] // 2, own.shape[1])
+    passed_a, passed_b = call(
+        halves_kernel,
+        [(half, own.dtype)] * 2,
+        [pltpu.SemaphoreType.DMA((2,))],
+        left,
+        right,
+        there=(0, 1),
+        limit=4 << 20,
+    )
     far_a = turn(passed_a, 1)
-    passed_b = right[half:]
     far_b = turn(passed_b, -1)
-    return (own, left, right, far_a, far_b), (passed_a, passed_b)
+    return (own, left, right, far_a, far_b), (passed_a, passed_b), earlier
 
 
 def on_device(
@@ -271,7 +300,6 @@
     hidden = gate_weight.shape[2]
     rows = slots * sources
 
-    w_down, passed = gathered(down_weight[0])
 
     packed = portion * width // 128
     (piece,) = call(
@@ -288,27 +316,17 @@
         routes.T,
         route_weight.T,
         out_grad,
-        there=True,
+        there=(1, 2, 3),
+        limit=67_000_000,
     )
     arrived = lax.all_to_all(
         piece.reshape(experts, packed, 128), "sp", split_axis=0, concat_axis=0, tiled=True
     )
 
-    in_gate, conv_input, out_gate, early_grad, out_weight = lax.optimization_barrier(
-        (in_gate, conv_input, out_gate, out_grad, out_weight, piece, *passed)
-    )[:5]
-    own_cols = lax.dynamic_slice_in_dim(early_grad, member * share, share, 1)
-    reach = taps.shape[0] - 1
-    mixed = in_gate.astype(F32) * conv_input.astype(F32)
-    prior_mixed = passed_along(mixed[tok_rows - reach :], "sp", 1)
-    extended = jnp.concatenate([prior_mixed, mixed], axis=0)
-    conv = jnp.zeros_like(mixed)
-    for tap in range(reach + 1):
-        conv = conv + taps[tap][None, :] * extended[reach - tap : reach - tap + tok_rows]
-    gated = (out_gate.astype(F32) * conv).astype(BF16)
-    gated_all = jnp.stack([gated, turn(gated, -1), turn(gated, 2), turn(gated, 1)])
-    out_weight_twice = jnp.concatenate([out_weight, out_weight], axis=0)
+    out_weight_twice = after(out_weight, piece)
+    out_weight_twice = jnp.concatenate([out_weight_twice, out_weight_twice], axis=0)
     out_weight_rel = lax.dynamic_slice_in_dim(out_weight_twice, member * share, width, 0)
+    w_down, passed, (out_weight_rel,) = gathered(down_weight[0], out_weight_rel)
 
     inputs = expert_rows[:, 0].transpose(1, 0, 2).reshape(rows, width)
     inputs = after(inputs, *passed)
@@ -319,32 +337,32 @@
     act = (gate * sig * up).astype(BF16)
     up_of = gate * sig
     gate_of = up * sig * (1.0 + gate * (1.0 - sig))
-    act_twice = act.reshape(groups, rows // groups, hidden)
-    act_twice = jnp.concatenate([act_twice, act_twice], axis=0)
-    act_rel = lax.dynamic_slice_in_dim(act_twice, member, groups, 0)
+    act = act.reshape(groups, rows // groups, hidden)
     (
-        arrived, up_of, gate_of, act_rel, gated_all, out_weight_rel, conv, own_cols
+        arrived, up_of, gate_of, act, out_weight_rel
     ) = lax.optimization_barrier(
-        (arrived, up_of, gate_of, act_rel, gated_all, out_weight_rel, conv, own_cols)
+        (arrived, up_of, gate_of, act, out_weight_rel)
     )
 
     block = portion * sources
     grads, *partial = call(
         arrive_kernel,
-        [((block, width), BF16)] + [((block, hidden), BF16)] * 4,
+        [((block, width), BF16)] + [((block, hidden), BF16)] * 3,
         [
             pltpu.VMEM((sources * packed, 128), F32),
             pltpu.VMEM((sources * packed, 128), BF16),
-            *[pltpu.VMEM((hidden, width), BF16)] * 4,
-            pltpu.SemaphoreType.DMA((6,)),
+            *[pltpu.VMEM((hidden, width), BF16)] * 3,
+            pltpu.SemaphoreType.DMA((4,)),
         ],
         arrived.reshape(sources * packed, 128),
-        *w_down,
-        there=True,
-    )
-    from_far = turn(partial[3], 2)
+        *w_down[:3],
+        there=(0, 1, 2, 3),
+        limit=65_200_000,
+    )
     from_left = turn(partial[2], 1)
     from_right = turn(partial[1], -1)
+    (partial_far,) = call(far_kernel, [((block, hidden), BF16)], [], grads, w_down[3], w_down[4])
+    from_far = turn(partial_far, 2)
     half = rows // 2
     gate_part, up_part, far_a, far_b = call(
         parts_kernel,
@@ -378,6 +396,22 @@
     prev_b = (prev_b.astype(F32) + far_b.astype(F32)).astype(BF16)
     left_a = turn(next_a, 1)
     right_b = turn(prev_b, -1)
+
+    in_gate, conv_input, out_gate = lax.optimization_barrier(
+        (in_gate, conv_input, out_gate, next_a, prev_b)
+    )[:3]
+    reach = taps.shape[0] - 1
+    mixed = in_gate.astype(F32) * conv_input.astype(F32)
+    prior_mixed = passed_along(mixed[tok_rows - reach :], "sp", 1)
+    extended = jnp.concatenate([prior_mixed, mixed], axis=0)
+    conv = jnp.zeros_like(mixed)
+    for tap in range(reach + 1):
+        conv = conv + taps[tap][None, :] * extended[reach - tap : reach - tap + tok_rows]
+    gated = (out_gate.astype(F32) * conv).astype(BF16)
+    gate_grad, up_grad = weight_grads(inputs, gate_part, up_part)
+    left_a, right_b, conv, gated, gate_grad, up_grad = lax.optimization_barrier(
+        (left_a, right_b, conv, gated, gate_grad, up_grad)
+    )
     (leaving,) = call(
         leave_kernel,
         [((experts * packed, 128), BF16)],
@@ -392,12 +426,14 @@
         leaving.reshape(sources, packed, 128), "sp", split_axis=0, concat_axis=0, tiled=True
     )
 
-    every, passed = gathered(after(grads, next_a, prev_b))
-    gate_grad, up_grad = weight_grads(inputs, gate_part, up_part)
-    (down_grad,) = call(down_kernel, [((hidden, width), BF16)], [], act_rel, *every)
-    returned, gate_grad, up_grad, down_grad = lax.optimization_barrier(
-        (returned, gate_grad, up_grad, down_grad)
-    )
+    every, passed, _ = gathered(after(grads, next_a, prev_b))
+    gated = after(gated, leaving)
+    gated_right = turn(gated, -1)
+    gated_far = turn(gated, 2)
+    gated_left = turn(gated, 1)
+    gated_all = jnp.stack([gated, gated_right, gated_far, gated_left])
+    (down_grad,) = call(down_kernel, [((hidden, width), BF16)], [], member[None], act, *every)
+    returned, gated_all = lax.optimization_barrier((returned, gated_all))
 
     core = lax.rem(lax.axis_index("sp"), 2)
     side = share // 2
@@ -408,12 +444,17 @@
             ((groups, side, hidden), BF16),
             ((groups, side, hidden), F32),
         ],
-        [pltpu.VMEM((experts * packed, 128), F32)],
-        core[None],
+        [
+            pltpu.VMEM((experts * packed, 128), F32),
+            pltpu.VMEM((tok_rows, share), BF16),
+            pltpu.SemaphoreType.DMA,
+        ],
+        jnp.stack([member, core]),
         routes.T,
         returned.reshape(experts * packed, 128),
-        own_cols,
+        out_grad,
         gated_all,
+        there=(3,),
     )
     swapped = lax.ppermute(sent, "sp", [(i, i ^ 1) for i in range(sources)])
 

time: 200 us -> 178 us (0.89)
  the two profiles are of different devices: /device:TPU:15 before, /device:TPU:20 now
where the time goes in v1:
time: 178 us
  starting transfers between devices  71.9 us (40%)
  waiting for transfers between devices  66 us (37%)
  Pallas kernels  23.7 us (13%)
  other arithmetic  6.62 us (4%)
  matrix products  5.52 us (3%)
  local copies, waits for them, and re-layouts  2.95 us (2%)
    ppermute x23, starting transfers between devices, turn(): lax.ppermute(shard, 'tp', [(i, (i + by) % peers) for i in range(peers)])  39.5 us
    ppermute x23, waiting for transfers between devices, turn(): lax.ppermute(shard, 'tp', [(i, (i + by) % peers) for i in range(peers)])  37.2 us
    pallas_call x10, Pallas kernels, call(): pl.pallas_call(kernel, out_shape=[jax.ShapeDtypeStruct(*o) for o in outs]...  20.1 us
    all_to_all x1, starting transfers between devices, on_device(): lax.all_to_all(piece.reshape(experts, packed, 128), 'sp', split_axis=0, c...  12.3 us
    all_to_all x1, waiting for transfers between devices, on_device(): lax.all_to_all(leaving.reshape(sources, packed, 128), 'sp', split_axis=0,...  12.2 us
    ppermute x1, waiting for transfers between devices, on_device(): out_weight_grad = lax.ppermute(out_weight_sum, ('sp', 'tp'), pairs)  9.72 us
    all_to_all x1, starting transfers between devices, on_device(): lax.all_to_all(leaving.reshape(sources, packed, 128), 'sp', split_axis=0,...  7.63 us
    all_to_all x1, waiting for transfers between devices, on_device(): lax.all_to_all(piece.reshape(experts, packed, 128), 'sp', split_axis=0, c...  6.87 us
  transfers between devices with their start and end apart: 30, of which 15 were waited for; matrix products, arithmetic and copies ran while one was open for 7% of the time, Pallas kernels for 11%

profile of v1, /device:TPU:20, one launch (start us, length us, event | category | flops | bytes accessed | tf_op | source)
XLA Modules:
  0.0 177.7 jit_solution(4840021190733464647)
XLA Ops:
  1.2 1.5 collective-permute-start
  2.7 2.8 %shard_map.179 = bf16[3072,128]{1,0:T(8,128)(2,1)} custom-call(s32[1]{0:T(128)} %bitcast.1.first_ref, s32[2,192]{1,0:T(2,128)} %bitcast.47, f32[2,192]{1,0:T(2,128)} %bitcast.64, bf16[192,2048]{1,0:T(8,128)(2,1)} %tokens_hbm.3), custom_call_target="tpu_custom_call" | custom-call | tf_op jit(solution)/shard_map/pallas_call | solution.py:234
  5.5 12.3 %all-to-all-start = ((bf16[64,48,128]{2,1,0:T(8,128)(2,1)}), bf16[64,48,128]{2,1,0:T(8,128)(2,1)}, u32[]{:S(2)}, u32[]{:S(2)}) async-start(bf16[64,48,128]{2,1,0:T(8,128)(2,1)} %bitcast.49), calls=%async_computation | async-start | bytes 1572864 | tf_op jit(solution)/shard_map/all_to_all | solution.py:322
  17.9 3.8 %fusion = bf16[2048,256]{1,0:T(8,128)(2,1)} fusion(s32[]{:T(128)S(6)} %select_n.3, bf16[2048,256]{1,0:T(8,128)(2,1)S(1)} %copy-done.12), kind=kLoop, calls=%fused_computation.2 | loop fusion | flops 2097152 | bytes 2097156 | tf_op jit(solution)/shard_map/concatenate | solution.py:327
  21.7 4.3 %collective-permute-done.1.right.w2_hbm = bf16[256,2048]{1,0:T(8,128)(2,1)} collective-permute-done((bf16[256,2048]{1,0:T(8,128)(2,1)}, bf16[256,2048]{1,0:T(8,128)(2,1)}, u32[]{:S(2)}, u32[]{:S(2)}) %collective-permute-start.1) | collective-permute-done | bytes 1048608 | tf_op jit(solution)/shard_map/ppermute | solution.py:246
  26.2 2.2 %shard_map.180 = (bf16[128,2048]{1,0:T(8,128)(2,1)}, bf16[128,2048]{1,0:T(8,128)(2,1)}) custom-call(bf16[256,2048]{1,0:T(8,128)(2,1)} %collective-permute-done.left.w1_hbm, bf16[256,2048]{1,0:T(8,128)(2,1)} %collective-permute-done.1.right.w2_hbm), custom_call_target="tpu_custom_call" | custom-call | tf_op jit(solution)/shard_map/pallas_call | solution.py:234
  28.4 2.2 %collective-permute-start.3 = (bf16[128,2048]{1,0:T(8,128)(2,1)}, bf16[128,2048]{1,0:T(8,128)(2,1)}, u32[]{:S(2)}, u32[]{:S(2)}) collective-permute-start(bf16[128,2048]{1,0:T(8,128)(2,1)} %get-tuple-element.58), channel_id=1, source_target_pairs={{0,1},{1,2},{2,3},{3,0},{4,5},{5,6},{6,7},{7,4},{8,9},{9,10},{10,1... | collective-permute-start | bytes 1572872 | tf_op jit(solution)/shard_map/ppermute | solution.py:246
  30.7 1.0 fusion.26
  31.9 2.2 %multiply_convert_fusion = (bf16[768,256]{1,0:T(8,128)(2,1)}, f32[768,256]{1,0:T(8,128)S(1)}, f32[768,256]{1,0:T(8,128)}) fusion(f32[768,256]{1,0:T(8,128)S(1)} %fusion.26, bf16[768,2048]{1,0:T(8,128)(2,1)S(1)} %bitcast.44, bf16[1,2048,256]{2,1,0:T(8,128)(2,1)S(1)} %copy-done.1), kind=kOutput, calls=%fused_computation.15 | convolution fusion | flops 807469056 | bytes 6946816 | tf_op jit(solution)/shard_map/dot_general | solution.py:14
  34.1 6.9 %all-to-all-done = bf16[64,48,128]{2,1,0:T(8,128)(2,1)} async-done(((bf16[64,48,128]{2,1,0:T(8,128)(2,1)}), bf16[64,48,128]{2,1,0:T(8,128)(2,1)}, u32[]{:S(2)}, u32[]{:S(2)}) %all-to-all-start) | async-done | bytes 786464 | tf_op jit(solution)/shard_map/all_to_all | solution.py:322
  40.9 4.4 %shard_map.181 = (bf16[192,2048]{1,0:T(8,128)(2,1)}, bf16[192,256]{1,0:T(8,128)(2,1)}, bf16[192,256]{1,0:T(8,128)(2,1)}, bf16[192,256]{1,0:T(8,128)(2,1)}) custom-call(bf16[3072,128]{1,0:T(8,128)(2,1)} %bitcast.12.arrived_hbm, bf16[256,2048]{1,0:T(8,128)(2,1)} %bitcast.53, bf16[256,2048]{1,0:T(8,128)(2,1)} %collective-permute-done.left.w1_hbm, ...), custom_call_target="tpu_custom_call" | custom-call | tf_op jit(solution)/shard_map/pallas_call | solution.py:234
  46.1 2.0 %collective-permute-start.6 = (bf16[192,256]{1,0:T(8,128)(2,1)}, bf16[192,256]{1,0:T(8,128)(2,1)S(1)}, u32[]{:S(2)}, u32[]{:S(2)}) collective-permute-start(bf16[192,256]{1,0:T(8,128)(2,1)} %get-tuple-element.66), channel_id=1, source_target_pairs={{0,1},{1,2},{2,3},{3,0},{4,5},{5,6},{6,7},{7,4},{8,9},{9,10},{10,1... | collective-permute-start | bytes 294920 | tf_op jit(solution)/shard_map/ppermute | solution.py:246
  48.1 1.1 copy-done.4
  49.2 1.8 %shard_map.182 = bf16[192,256]{1,0:T(8,128)(2,1)S(1)} custom-call(bf16[192,2048]{1,0:T(8,128)(2,1)S(1)} %copy-done.4, bf16[128,2048]{1,0:T(8,128)(2,1)} %collective-permute-done.3.w3a, bf16[128,2048]{1,0:T(8,128)(2,1)} %collective-permute-done.4.w3b), custom_call_target="tpu_custom_call" | custom-call | tf_op jit(solution)/shard_map/pallas_call | solution.py:234
  51.1 2.1 %collective-permute-start.5 = (bf16[192,256]{1,0:T(8,128)(2,1)S(1)}, bf16[192,256]{1,0:T(8,128)(2,1)S(1)}, u32[]{:S(2)}, u32[]{:S(2)}) collective-permute-start(bf16[192,256]{1,0:T(8,128)(2,1)S(1)} %shard_map.182), channel_id=1, source_target_pairs={{0,2},{1,3},{2,0},{3,1},{4,6},{5,7},{6,4},{7,5},{8,10},{9,11},{10,... | collective-permute-start | bytes 294920 | tf_op jit(solution)/shard_map/ppermute | solution.py:246
  53.2 4.1 %collective-permute-done.5.far = bf16[192,256]{1,0:T(8,128)(2,1)S(1)} collective-permute-done((bf16[192,256]{1,0:T(8,128)(2,1)S(1)}, bf16[192,256]{1,0:T(8,128)(2,1)S(1)}, u32[]{:S(2)}, u32[]{:S(2)}) %collective-permute-start.5) | collective-permute-done | bytes 98336 | tf_op jit(solution)/shard_map/ppermute | solution.py:246
  58.9 1.2 collective-permute-start.9
  60.0 2.1 %collective-permute-start.7 = (bf16[384,512]{1,0:T(8,128)(2,1)S(1)}, bf16[384,512]{1,0:T(8,128)(2,1)S(1)}, u32[]{:S(2)}, u32[]{:S(2)}) collective-permute-start(bf16[384,512]{1,0:T(8,128)(2,1)S(1)} %get-tuple-element.72), channel_id=1, source_target_pairs={{0,1},{1,2},{2,3},{3,0},{4,5},{5,6},{6,7},{7,4},{8,9},{9,10},{10,1... | collective-permute-start | bytes 1179656 | tf_op jit(solution)/shard_map/ppermute | solution.py:246
  62.2 1.4 shard_map.184
  63.7 3.2 %collective-permute-start.17 = (bf16[384,512]{1,0:T(8,128)(2,1)S(1)}, bf16[384,512]{1,0:T(8,128)(2,1)S(1)}, u32[]{:S(2)}, u32[]{:S(2)}) collective-permute-start(bf16[384,512]{1,0:T(8,128)(2,1)S(1)} %get-tuple-element.91), channel_id=1, source_target_pairs={{0,1},{1,2},{2,3},{3,0},{4,5},{5,6},{6,7},{7,4},{8,9},{9,10},{10,1... | collective-permute-start | bytes 1179656 | tf_op jit(solution)/shard_map/ppermute | solution.py:246
  66.9 5.1 %collective-permute-done.9 = bf16[384,512]{1,0:T(8,128)(2,1)S(1)} collective-permute-done((bf16[384,512]{1,0:T(8,128)(2,1)S(1)}, bf16[384,512]{1,0:T(8,128)(2,1)S(1)}, u32[]{:S(2)}, u32[]{:S(2)}) %collective-permute-start.9) | collective-permute-done | bytes 393248 | tf_op jit(solution)/shard_map/ppermute | solution.py:246
  72.4 3.3 %collective-permute-start.8 = (bf16[384,512]{1,0:T(8,128)(2,1)S(1)}, bf16[384,512]{1,0:T(8,128)(2,1)S(1)}, u32[]{:S(2)}, u32[]{:S(2)}) collective-permute-start(bf16[384,512]{1,0:T(8,128)(2,1)S(1)} %add_convert_fusion.2), channel_id=1, source_target_pairs={{0,1},{1,2},{2,3},{3,0},{4,5},{5,6},{6,7},{7,4},{8,9},{9,10},{10,1... | collective-permute-start | bytes 1179656 | tf_op jit(solution)/shard_map/ppermute | solution.py:246
  75.7 1.9 %collective-permute-start.11 = (f32[2,256]{1,0:T(2,128)S(1)}, f32[2,256]{1,0:T(2,128)S(1)}, u32[]{:S(2)}, u32[]{:S(2)}) collective-permute-start(f32[2,256]{1,0:T(2,128)S(1)} %slice.39), channel_id=1, source_target_pairs={{0,4},{4,8},{8,12},{12,16},{16,20},{20,24},{24,28},{28,32},{32,36}... | collective-permute-start | bytes 6152 | tf_op jit(solution)/shard_map/ppermute | solution.py:252
  77.7 3.6 %weights.1 = (bf16[2048,256]{1,0:T(8,128)(2,1)}, bf16[2048,256]{1,0:T(8,128)(2,1)}) custom-call(bf16[768,2048]{1,0:T(8,128)(2,1)S(1)} %bitcast.45, bf16[768,256]{1,0:T(8,128)(2,1)S(1)} %get-tuple-element.69.gate_part, bf16[768,256]{1,0:T(8,128)(2,1)S(1)} %get-tuple-element.70.up_part), custom_call_target="tpu_custom_call" | custom-call | tf_op jit(solution)/shard_map/weights/pallas_call | solution.py:219
  81.4 3.8 %collective-permute-done.10.right_b = bf16[384,512]{1,0:T(8,128)(2,1)S(1)} collective-permute-done((bf16[384,512]{1,0:T(8,128)(2,1)S(1)}, bf16[384,512]{1,0:T(8,128)(2,1)S(1)}, u32[]{:S(2)}, u32[]{:S(2)}) %collective-permute-start.10) | collective-permute-done | bytes 393248 | tf_op jit(solution)/shard_map/ppermute | solution.py:246
  85.2 1.5 shard_map.187
  86.8 7.6 %all-to-all-start.1 = ((bf16[64,48,128]{2,1,0:T(8,128)(2,1)}), bf16[64,48,128]{2,1,0:T(8,128)(2,1)S(1)}, u32[]{:S(2)}, u32[]{:S(2)}) async-start(bf16[64,48,128]{2,1,0:T(8,128)(2,1)} %bitcast.20), calls=%async_computation.1 | async-start | bytes 1572864 | tf_op jit(solution)/shard_map/all_to_all | solution.py:425
  94.4 3.0 %collective-permute-start.20 = (bf16[192,256]{1,0:T(8,128)(2,1)S(1)}, bf16[192,256]{1,0:T(8,128)(2,1)S(1)}, u32[]{:S(2)}, u32[]{:S(2)}) collective-permute-start(bf16[192,256]{1,0:T(8,128)(2,1)S(1)} %get-tuple-element.94), channel_id=1, source_target_pairs={{0,1},{1,2},{2,3},{3,0},{4,5},{5,6},{6,7},{7,4},{8,9},{9,10},{10,1... | collective-permute-start | bytes 294920 | tf_op jit(solution)/shard_map/ppermute | solution.py:246
  97.5 1.9 %collective-permute-start.19 = (bf16[192,256]{1,0:T(8,128)(2,1)S(1)}, bf16[192,256]{1,0:T(8,128)(2,1)S(1)}, u32[]{:S(2)}, u32[]{:S(2)}) collective-permute-start(bf16[192,256]{1,0:T(8,128)(2,1)S(1)} %get-tuple-element.94), channel_id=1, source_target_pairs={{0,2},{1,3},{2,0},{3,1},{4,6},{5,7},{6,4},{7,5},{8,10},{9,11},{10,... | collective-permute-start | bytes 294920 | tf_op jit(solution)/shard_map/ppermute | solution.py:246
  99.3 2.5 %collective-permute-start.18 = (bf16[192,256]{1,0:T(8,128)(2,1)S(1)}, bf16[192,256]{1,0:T(8,128)(2,1)S(1)}, u32[]{:S(2)}, u32[]{:S(2)}) collective-permute-start(bf16[192,256]{1,0:T(8,128)(2,1)S(1)} %get-tuple-element.94), channel_id=1, source_target_pairs={{0,3},{1,0},{2,1},{3,2},{4,7},{5,4},{6,5},{7,6},{8,11},{9,8},{10,9... | collective-permute-start | bytes 294920 | tf_op jit(solution)/shard_map/ppermute | solution.py:246
  102.0 2.5 %collective-permute-done.19 = bf16[192,256]{1,0:T(8,128)(2,1)S(1)} collective-permute-done((bf16[192,256]{1,0:T(8,128)(2,1)S(1)}, bf16[192,256]{1,0:T(8,128)(2,1)S(1)}, u32[]{:S(2)}, u32[]{:S(2)}) %collective-permute-start.19) | collective-permute-done | bytes 98336 | tf_op jit(solution)/shard_map/ppermute | solution.py:246
  105.4 12.2 %all-to-all-done.1 = bf16[64,48,128]{2,1,0:T(8,128)(2,1)S(1)} async-done(((bf16[64,48,128]{2,1,0:T(8,128)(2,1)}), bf16[64,48,128]{2,1,0:T(8,128)(2,1)S(1)}, u32[]{:S(2)}, u32[]{:S(2)}) %all-to-all-start.1) | async-done | bytes 786464 | tf_op jit(solution)/shard_map/all_to_all | solution.py:425
  117.6 2.4 %shard_map.188 = (bf16[192,512]{1,0:T(8,128)(2,1)}, bf16[4,256,256]{2,1,0:T(8,128)(2,1)S(1)}, f32[4,256,256]{2,1,0:T(8,128)S(1)}) custom-call(s32[2]{0:T(128)S(1)} %pad_add_fusion.where_ref, s32[2,192]{1,0:T(2,128)S(1)} %bitcast.48, bf16[3072,128]{1,0:T(8,128)(2,1)S(1)} %bitcast.42, bf16[192,2048]{1,0:T(8,128)(2,1)S(1)} %copy-done.3, ...), custom_call_target="tpu_custom_call" | custom-call | tf_op jit(solution)/shard_map/pallas_call | solution.py:234
  120.1 2.4 %collective-permute-start.13 = (bf16[192,2048]{1,0:T(8,128)(2,1)S(1)}, bf16[192,2048]{1,0:T(8,128)(2,1)S(1)}, u32[]{:S(2)}, u32[]{:S(2)}) collective-permute-start(bf16[192,2048]{1,0:T(8,128)(2,1)S(1)} %copy-done.5), channel_id=1, source_target_pairs={{0,3},{1,0},{2,1},{3,2},{4,7},{5,4},{6,5},{7,6},{8,11},{9,8},{10,9... | collective-permute-start | bytes 2359304 | tf_op jit(solution)/shard_map/ppermute | solution.py:246
  124.1 5.3 %all-to-all-start.2 = ((bf16[32,32,256]{2,1,0:T(8,128)(2,1)}), bf16[32,32,256]{2,1,0:T(8,128)(2,1)S(1)}, u32[]{:S(2)}, u32[]{:S(2)}) async-start(bf16[32,32,256]{2,1,0:T(8,128)(2,1)} %bitcast.26), calls=%async_computation.2 | async-start | bytes 1048576 | tf_op jit(solution)/shard_map/all_to_all | solution.py:468
  129.5 3.2 %collective-permute-start.25 = (bf16[192,512]{1,0:T(8,128)(2,1)}, bf16[192,512]{1,0:T(8,128)(2,1)S(1)}, u32[]{:S(2)}, u32[]{:S(2)}) collective-permute-start(bf16[192,512]{1,0:T(8,128)(2,1)} %get-tuple-element.125), channel_id=1, source_target_pairs={{0,1},{1,2},{2,3},{3,0},{4,5},{5,6},{6,7},{7,4},{8,9},{9,10},{10,1... | collective-permute-start | bytes 589832 | tf_op jit(solution)/shard_map/ppermute | solution.py:246
  133.4 2.5 %collective-permute-start.23 = (bf16[192,512]{1,0:T(8,128)(2,1)}, bf16[192,512]{1,0:T(8,128)(2,1)S(1)}, u32[]{:S(2)}, u32[]{:S(2)}) collective-permute-start(bf16[192,512]{1,0:T(8,128)(2,1)} %get-tuple-element.125), channel_id=1, source_target_pairs={{0,3},{1,0},{2,1},{3,2},{4,7},{5,4},{6,5},{7,6},{8,11},{9,8},{10,9... | collective-permute-start | bytes 589832 | tf_op jit(solution)/shard_map/ppermute | solution.py:246
  135.9 5.6 %collective-permute-done.13.right.g2 = bf16[192,2048]{1,0:T(8,128)(2,1)S(1)} collective-permute-done((bf16[192,2048]{1,0:T(8,128)(2,1)S(1)}, bf16[192,2048]{1,0:T(8,128)(2,1)S(1)}, u32[]{:S(2)}, u32[]{:S(2)}) %collective-permute-start.13) | collective-permute-done | bytes 786464 | tf_op jit(solution)/shard_map/ppermute | solution.py:246
  141.5 2.3 %collective-permute-done.12.left.g1 = bf16[192,2048]{1,0:T(8,128)(2,1)S(1)} collective-permute-done((bf16[192,2048]{1,0:T(8,128)(2,1)S(1)}, bf16[192,2048]{1,0:T(8,128)(2,1)S(1)}, u32[]{:S(2)}, u32[]{:S(2)}) %collective-permute-start.12) | collective-permute-done | bytes 786464 | tf_op jit(solution)/shard_map/ppermute | solution.py:246
  144.2 1.0 collective-permute-start.14
  145.2 2.4 %collective-permute-start.15 = (bf16[96,2048]{1,0:T(8,128)(2,1)S(1)}, bf16[96,2048]{1,0:T(8,128)(2,1)S(1)}, u32[]{:S(2)}, u32[]{:S(2)}) collective-permute-start(bf16[96,2048]{1,0:T(8,128)(2,1)S(1)} %get-tuple-element.87), channel_id=1, source_target_pairs={{0,3},{1,0},{2,1},{3,2},{4,7},{5,4},{6,5},{7,6},{8,11},{9,8},{10,9... | collective-permute-start | bytes 1179656 | tf_op jit(solution)/shard_map/ppermute | solution.py:246
  148.3 5.5 %collective-permute-done.24 = bf16[192,512]{1,0:T(8,128)(2,1)S(1)} collective-permute-done((bf16[192,512]{1,0:T(8,128)(2,1)}, bf16[192,512]{1,0:T(8,128)(2,1)S(1)}, u32[]{:S(2)}, u32[]{:S(2)}) %collective-permute-start.24) | collective-permute-done | bytes 196640 | tf_op jit(solution)/shard_map/ppermute | solution.py:246
  153.8 2.4 %multiply_convert_fusion.1 = (bf16[192,256]{1,0:T(8,128)(2,1)}, f32[192,256]{1,0:T(8,128)S(1)}) fusion(f32[192,256]{1,0:T(8,128)S(1)} %get-tuple-element.101, bf16[192,256]{1,0:T(8,128)(2,1)S(1)} %copy-done.15, bf16[2048,256]{1,0:T(8,128)(2,1)} %fusion, bf16[192,512]{1,0:T(8,128)(2,1)S(1)} %collective-permute-done.25, ...), kind=kOutput, calls=%fused_computation.44 | convolution fusion | flops 204668928 | bytes 2424832 | tf_op jit(solution)/shard_map/dot_general | solution.py:14
  156.1 1.9 %collective-permute-start.26 = (f32[2,256]{1,0:T(2,128)S(1)}, f32[2,256]{1,0:T(2,128)S(1)}, u32[]{:S(2)}, u32[]{:S(2)}) collective-permute-start(f32[2,256]{1,0:T(2,128)S(1)} %slice.42), channel_id=1, source_target_pairs={{4,0},{8,4},{12,8},{16,12},{20,16},{24,20},{28,24},{32,28},{36,32}... | collective-permute-start | bytes 6152 | tf_op jit(solution)/shard_map/ppermute | solution.py:252
  158.1 2.1 %collective-permute-done.14.g3a = bf16[96,2048]{1,0:T(8,128)(2,1)S(1)} collective-permute-done((bf16[96,2048]{1,0:T(8,128)(2,1)S(1)}, bf16[96,2048]{1,0:T(8,128)(2,1)S(1)}, u32[]{:S(2)}, u32[]{:S(2)}) %collective-permute-start.14) | collective-permute-done | bytes 393248 | tf_op jit(solution)/shard_map/ppermute | solution.py:246
  160.1 2.5 %shard_map.186 = bf16[256,2048]{1,0:T(8,128)(2,1)} custom-call(s32[1]{0:T(128)} %bitcast.member_ref, bf16[4,192,256]{2,1,0:T(8,128)(2,1)S(1)} %bitcast.46, bf16[192,2048]{1,0:T(8,128)(2,1)S(1)} %copy-done.5, bf16[192,2048]{1,0:T(8,128)(2,1)S(1)} %collective-permute-done.12.left.g1, bf16[192,2048]{1,0:T(8,128)(2,1)S(1)} %collective-permute-done.13.right.g2, ...), custom_call_target="tpu_custom_call" | custom-call | tf_op jit(solution)/shard_map/pallas_call | solution.py:234
  163.5 3.2 %collective-permute-start.22 = (f32[32,256]{1,0:T(8,128)S(1)}, f32[32,256]{1,0:T(8,128)S(1)}, u32[]{:S(2)}, u32[]{:S(2)}) collective-permute-start(f32[32,256]{1,0:T(8,128)S(1)} %convert_reduce_fusion), channel_id=1, source_target_pairs={{0,0},{1,65},{2,130},{3,195},{4,32},{5,97},{6,162},{7,227},{8,4},{... | collective-permute-start | bytes 98312 | tf_op jit(solution)/shard_map/ppermute | solution.py:484
  167.4 9.7 %collective-permute-done.22 = f32[32,256]{1,0:T(8,128)S(1)} collective-permute-done((f32[32,256]{1,0:T(8,128)S(1)}, f32[32,256]{1,0:T(8,128)S(1)}, u32[]{:S(2)}, u32[]{:S(2)}) %collective-permute-start.22) | collective-permute-done | bytes 32800 | tf_op jit(solution)/shard_map/ppermute | solution.py:484
  (75 shorter events, 10.5 us)
Async XLA Ops:
  0.6 25.3 %collective-permute-start.1 = (bf16[256,2048]{1,0:T(8,128)(2,1)}, bf16[256,2048]{1,0:T(8,128)(2,1)}, u32[]{:S(2)}, u32[]{:S(2)}) collective-permute-start(bf16[256,2048]{1,0:T(8,128)(2,1)} %bitcast.51), channel_id=1, source_target_pairs={{0,3},{1,0},{2,1},{3,2},{4,7},{5,4},{6,5},{7,6},{8,11},{9,8},{10,9... | collective-permute-start | bytes 3145736 | tf_op jit(solution)/shard_map/ppermute | solution.py:246
  1.2 24.9 %collective-permute-start = (bf16[256,2048]{1,0:T(8,128)(2,1)}, bf16[256,2048]{1,0:T(8,128)(2,1)}, u32[]{:S(2)}, u32[]{:S(2)}) collective-permute-start(bf16[256,2048]{1,0:T(8,128)(2,1)} %bitcast.52), channel_id=1, source_target_pairs={{0,1},{1,2},{2,3},{3,0},{4,5},{5,6},{6,7},{7,4},{8,9},{9,10},{10,1... | collective-permute-start | bytes 3145736 | tf_op jit(solution)/shard_map/ppermute | solution.py:246
  5.5 12.3 %copy-start.12 = (bf16[2048,256]{1,0:T(8,128)(2,1)S(1)}, bf16[2048,256]{1,0:T(8,128)(2,1)}, u32[]{:S(2)}) copy-start(bf16[2048,256]{1,0:T(8,128)(2,1)} %param.23) | copy-start | bytes 3145732
  5.5 35.4 %all-to-all-start = ((bf16[64,48,128]{2,1,0:T(8,128)(2,1)}), bf16[64,48,128]{2,1,0:T(8,128)(2,1)}, u32[]{:S(2)}, u32[]{:S(2)}) async-start(bf16[64,48,128]{2,1,0:T(8,128)(2,1)} %bitcast.49), calls=%async_computation | async-start | bytes 1572864 | tf_op jit(solution)/shard_map/all_to_all | solution.py:322
  17.8 12.8 %copy-start = (bf16[1,2048,256]{2,1,0:T(8,128)(2,1)S(1)}, bf16[1,2048,256]{2,1,0:T(8,128)(2,1)}, u32[]{:S(2)}) copy-start(bf16[1,2048,256]{2,1,0:T(8,128)(2,1)} %param.16) | copy-start | bytes 3145732
  17.8 12.8 %copy-start.6 = (bf16[64,1,12,2048]{3,0,2,1:T(8,128)(2,1)S(1)}, bf16[64,1,12,2048]{3,0,2,1:T(8,128)(2,1)}, u32[]{:S(2)}) copy-start(bf16[64,1,12,2048]{3,0,2,1:T(8,128)(2,1)} %param.15) | copy-start | bytes 9437188
  28.4 19.7 %collective-permute-start.3 = (bf16[128,2048]{1,0:T(8,128)(2,1)}, bf16[128,2048]{1,0:T(8,128)(2,1)}, u32[]{:S(2)}, u32[]{:S(2)}) collective-permute-start(bf16[128,2048]{1,0:T(8,128)(2,1)} %get-tuple-element.58), channel_id=1, source_target_pairs={{0,1},{1,2},{2,3},{3,0},{4,5},{5,6},{6,7},{7,4},{8,9},{9,10},{10,1... | collective-permute-start | bytes 1572872 | tf_op jit(solution)/shard_map/ppermute | solution.py:246
  30.6 17.5 %collective-permute-start.4 = (bf16[128,2048]{1,0:T(8,128)(2,1)}, bf16[128,2048]{1,0:T(8,128)(2,1)}, u32[]{:S(2)}, u32[]{:S(2)}) collective-permute-start(bf16[128,2048]{1,0:T(8,128)(2,1)} %get-tuple-element.59), channel_id=1, source_target_pairs={{0,3},{1,0},{2,1},{3,2},{4,7},{5,4},{6,5},{7,6},{8,11},{9,8},{10,9... | collective-permute-start | bytes 1572872 | tf_op jit(solution)/shard_map/ppermute | solution.py:246
  30.7 1.2 copy-start.1
  45.3 12.0 %copy-start.2 = (bf16[1,2048,256]{2,1,0:T(8,128)(2,1)S(1)}, bf16[1,2048,256]{2,1,0:T(8,128)(2,1)}, u32[]{:S(2)}) copy-start(bf16[1,2048,256]{2,1,0:T(8,128)(2,1)} %param.17) | copy-start | bytes 3145732
  45.4 7.8 %collective-permute-start.2 = (bf16[192,256]{1,0:T(8,128)(2,1)}, bf16[192,256]{1,0:T(8,128)(2,1)S(1)}, u32[]{:S(2)}, u32[]{:S(2)}) collective-permute-start(bf16[192,256]{1,0:T(8,128)(2,1)} %get-tuple-element.64), channel_id=1, source_target_pairs={{0,3},{1,0},{2,1},{3,2},{4,7},{5,4},{6,5},{7,6},{8,11},{9,8},{10,9... | collective-permute-start | bytes 294920 | tf_op jit(solution)/shard_map/ppermute | solution.py:246
  46.1 7.0 %collective-permute-start.6 = (bf16[192,256]{1,0:T(8,128)(2,1)}, bf16[192,256]{1,0:T(8,128)(2,1)S(1)}, u32[]{:S(2)}, u32[]{:S(2)}) collective-permute-start(bf16[192,256]{1,0:T(8,128)(2,1)} %get-tuple-element.66), channel_id=1, source_target_pairs={{0,1},{1,2},{2,3},{3,0},{4,5},{5,6},{6,7},{7,4},{8,9},{9,10},{10,1... | collective-permute-start | bytes 294920 | tf_op jit(solution)/shard_map/ppermute | solution.py:246
  48.1 1.1 copy-start.4
  49.2 8.1 %copy-start.8 = (f32[768,256]{1,0:T(8,128)S(1)}, f32[768,256]{1,0:T(8,128)}, u32[]{:S(2)}) copy-start(f32[768,256]{1,0:T(8,128)} %get-tuple-element.67.up_of) | copy-start | bytes 2359300
  51.1 6.2 %collective-permute-start.5 = (bf16[192,256]{1,0:T(8,128)(2,1)S(1)}, bf16[192,256]{1,0:T(8,128)(2,1)S(1)}, u32[]{:S(2)}, u32[]{:S(2)}) collective-permute-start(bf16[192,256]{1,0:T(8,128)(2,1)S(1)} %shard_map.182), channel_id=1, source_target_pairs={{0,2},{1,3},{2,0},{3,1},{4,6},{5,7},{6,4},{7,5},{8,10},{9,11},{10,... | collective-permute-start | bytes 294920 | tf_op jit(solution)/shard_map/ppermute | solution.py:246
  57.3 0.9 copy-start.10
  58.9 13.2 %collective-permute-start.9 = (bf16[384,512]{1,0:T(8,128)(2,1)S(1)}, bf16[384,512]{1,0:T(8,128)(2,1)S(1)}, u32[]{:S(2)}, u32[]{:S(2)}) collective-permute-start(bf16[384,512]{1,0:T(8,128)(2,1)S(1)} %get-tuple-element.74), channel_id=1, source_target_pairs={{0,3},{1,0},{2,1},{3,2},{4,7},{5,4},{6,5},{7,6},{8,11},{9,8},{10,9... | collective-permute-start | bytes 1179656 | tf_op jit(solution)/shard_map/ppermute | solution.py:246
  60.0 12.2 %collective-permute-start.7 = (bf16[384,512]{1,0:T(8,128)(2,1)S(1)}, bf16[384,512]{1,0:T(8,128)(2,1)S(1)}, u32[]{:S(2)}, u32[]{:S(2)}) collective-permute-start(bf16[384,512]{1,0:T(8,128)(2,1)S(1)} %get-tuple-element.72), channel_id=1, source_target_pairs={{0,1},{1,2},{2,3},{3,0},{4,5},{5,6},{6,7},{7,4},{8,9},{9,10},{10,1... | collective-permute-start | bytes 1179656 | tf_op jit(solution)/shard_map/ppermute | solution.py:246
  62.2 13.5 %copy-start.13 = (bf16[192,256]{1,0:T(8,128)(2,1)S(1)}, bf16[192,256]{1,0:T(8,128)(2,1)}, u32[]{:S(2)}) copy-start(bf16[192,256]{1,0:T(8,128)(2,1)} %param.19) | copy-start | bytes 294916
  62.2 13.5 %copy-start.14 = (bf16[192,256]{1,0:T(8,128)(2,1)S(1)}, bf16[192,256]{1,0:T(8,128)(2,1)}, u32[]{:S(2)}) copy-start(bf16[192,256]{1,0:T(8,128)(2,1)} %param.21) | copy-start | bytes 294916
  62.2 15.5 %copy-start.7 = (bf16[64,1,12,2048]{3,0,2,1:T(8,128)(2,1)S(1)}, bf16[64,1,12,2048]{3,0,2,1:T(8,128)(2,1)}, u32[]{:S(2)}) copy-start(bf16[64,1,12,2048]{3,0,2,1:T(8,128)(2,1)} %param.15) | copy-start | bytes 9437188
  63.6 14.0 %copy-start.16 = (f32[3,256]{1,0:T(4,128)S(1)}, f32[3,256]{1,0:T(4,128)}, u32[]{:S(2)}) copy-start(f32[3,256]{1,0:T(4,128)} %param.22) | copy-start | bytes 9220
  63.6 21.6 %collective-permute-start.16 = (bf16[384,512]{1,0:T(8,128)(2,1)S(1)}, bf16[384,512]{1,0:T(8,128)(2,1)S(1)}, u32[]{:S(2)}, u32[]{:S(2)}) collective-permute-start(bf16[384,512]{1,0:T(8,128)(2,1)S(1)} %get-tuple-element.90), channel_id=1, source_target_pairs={{0,3},{1,0},{2,1},{3,2},{4,7},{5,4},{6,5},{7,6},{8,11},{9,8},{10,9... | collective-permute-start | bytes 1179656 | tf_op jit(solution)/shard_map/ppermute | solution.py:246
  63.7 21.5 %collective-permute-start.17 = (bf16[384,512]{1,0:T(8,128)(2,1)S(1)}, bf16[384,512]{1,0:T(8,128)(2,1)S(1)}, u32[]{:S(2)}, u32[]{:S(2)}) collective-permute-start(bf16[384,512]{1,0:T(8,128)(2,1)S(1)} %get-tuple-element.91), channel_id=1, source_target_pairs={{0,1},{1,2},{2,3},{3,0},{4,5},{5,6},{6,7},{7,4},{8,9},{9,10},{10,1... | collective-permute-start | bytes 1179656 | tf_op jit(solution)/shard_map/ppermute | solution.py:246
  72.2 13.1 %collective-permute-start.10 = (bf16[384,512]{1,0:T(8,128)(2,1)S(1)}, bf16[384,512]{1,0:T(8,128)(2,1)S(1)}, u32[]{:S(2)}, u32[]{:S(2)}) collective-permute-start(bf16[384,512]{1,0:T(8,128)(2,1)S(1)} %add_convert_fusion.1), channel_id=1, source_target_pairs={{0,3},{1,0},{2,1},{3,2},{4,7},{5,4},{6,5},{7,6},{8,11},{9,8},{10,9... | collective-permute-start | bytes 1179656 | tf_op jit(solution)/shard_map/ppermute | solution.py:246
  72.4 9.0 %copy-start.15 = (bf16[192,256]{1,0:T(8,128)(2,1)S(1)}, bf16[192,256]{1,0:T(8,128)(2,1)}, u32[]{:S(2)}) copy-start(bf16[192,256]{1,0:T(8,128)(2,1)} %param.20) | copy-start | bytes 294916
  72.4 12.9 %collective-permute-start.8 = (bf16[384,512]{1,0:T(8,128)(2,1)S(1)}, bf16[384,512]{1,0:T(8,128)(2,1)S(1)}, u32[]{:S(2)}, u32[]{:S(2)}) collective-permute-start(bf16[384,512]{1,0:T(8,128)(2,1)S(1)} %add_convert_fusion.2), channel_id=1, source_target_pairs={{0,1},{1,2},{2,3},{3,0},{4,5},{5,6},{6,7},{7,4},{8,9},{9,10},{10,1... | collective-permute-start | bytes 1179656 | tf_op jit(solution)/shard_map/ppermute | solution.py:246
  75.7 5.6 %collective-permute-start.11 = (f32[2,256]{1,0:T(2,128)S(1)}, f32[2,256]{1,0:T(2,128)S(1)}, u32[]{:S(2)}, u32[]{:S(2)}) collective-permute-start(f32[2,256]{1,0:T(2,128)S(1)} %slice.39), channel_id=1, source_target_pairs={{0,4},{4,8},{8,12},{12,16},{16,20},{20,24},{24,28},{28,32},{32,36}... | collective-permute-start | bytes 6152 | tf_op jit(solution)/shard_map/ppermute | solution.py:252
  86.8 30.8 %copy-start.3 = (bf16[192,2048]{1,0:T(8,128)(2,1)S(1)}, bf16[192,2048]{1,0:T(8,128)(2,1)}, u32[]{:S(2)}) copy-start(bf16[192,2048]{1,0:T(8,128)(2,1)} %tokens_hbm.3) | copy-start | bytes 2359300
  86.8 30.8 %copy-start.11 = (s32[192,2]{0,1:T(2,128)S(1)}, s32[192,2]{0,1:T(2,128)}, u32[]{:S(2)}) copy-start(s32[192,2]{0,1:T(2,128)} %param.13) | copy-start | bytes 4612
  86.8 33.3 %copy-start.5 = (bf16[192,2048]{1,0:T(8,128)(2,1)S(1)}, bf16[192,2048]{1,0:T(8,128)(2,1)}, u32[]{:S(2)}) copy-start(bf16[192,2048]{1,0:T(8,128)(2,1)} %get-tuple-element.83.rows_ref.g0) | copy-start | bytes 2359300
  86.8 30.8 %all-to-all-start.1 = ((bf16[64,48,128]{2,1,0:T(8,128)(2,1)}), bf16[64,48,128]{2,1,0:T(8,128)(2,1)S(1)}, u32[]{:S(2)}, u32[]{:S(2)}) async-start(bf16[64,48,128]{2,1,0:T(8,128)(2,1)} %bitcast.20), calls=%async_computation.1 | async-start | bytes 1572864 | tf_op jit(solution)/shard_map/all_to_all | solution.py:425
  94.4 7.5 %collective-permute-start.20 = (bf16[192,256]{1,0:T(8,128)(2,1)S(1)}, bf16[192,256]{1,0:T(8,128)(2,1)S(1)}, u32[]{:S(2)}, u32[]{:S(2)}) collective-permute-start(bf16[192,256]{1,0:T(8,128)(2,1)S(1)} %get-tuple-element.94), channel_id=1, source_target_pairs={{0,1},{1,2},{2,3},{3,0},{4,5},{5,6},{6,7},{7,4},{8,9},{9,10},{10,1... | collective-permute-start | bytes 294920 | tf_op jit(solution)/shard_map/ppermute | solution.py:246
  97.5 7.0 %collective-permute-start.19 = (bf16[192,256]{1,0:T(8,128)(2,1)S(1)}, bf16[192,256]{1,0:T(8,128)(2,1)S(1)}, u32[]{:S(2)}, u32[]{:S(2)}) collective-permute-start(bf16[192,256]{1,0:T(8,128)(2,1)S(1)} %get-tuple-element.94), channel_id=1, source_target_pairs={{0,2},{1,3},{2,0},{3,1},{4,6},{5,7},{6,4},{7,5},{8,10},{9,11},{10,... | collective-permute-start | bytes 294920 | tf_op jit(solution)/shard_map/ppermute | solution.py:246
  99.3 6.0 %collective-permute-start.18 = (bf16[192,256]{1,0:T(8,128)(2,1)S(1)}, bf16[192,256]{1,0:T(8,128)(2,1)S(1)}, u32[]{:S(2)}, u32[]{:S(2)}) collective-permute-start(bf16[192,256]{1,0:T(8,128)(2,1)S(1)} %get-tuple-element.94), channel_id=1, source_target_pairs={{0,3},{1,0},{2,1},{3,2},{4,7},{5,4},{6,5},{7,6},{8,11},{9,8},{10,9... | collective-permute-start | bytes 294920 | tf_op jit(solution)/shard_map/ppermute | solution.py:246
  120.0 3.2 %collective-permute-start.21 = (bf16[4,256,256]{2,1,0:T(8,128)(2,1)S(1)}, bf16[4,256,256]{2,1,0:T(8,128)(2,1)S(1)}, u32[]{:S(2)}, u32[]{:S(2)}) collective-permute-start(bf16[4,256,256]{2,1,0:T(8,128)(2,1)S(1)} %get-tuple-element.99), channel_id=1, source_target_pairs={{0,4},{4,0},{8,12},{12,8},{16,20},{20,16},{24,28},{28,24},{32,36},... | collective-permute-start | bytes 1572872 | tf_op jit(solution)/shard_map/ppermute | solution.py:459
  120.1 21.4 %collective-permute-start.13 = (bf16[192,2048]{1,0:T(8,128)(2,1)S(1)}, bf16[192,2048]{1,0:T(8,128)(2,1)S(1)}, u32[]{:S(2)}, u32[]{:S(2)}) collective-permute-start(bf16[192,2048]{1,0:T(8,128)(2,1)S(1)} %copy-done.5), channel_id=1, source_target_pairs={{0,3},{1,0},{2,1},{3,2},{4,7},{5,4},{6,5},{7,6},{8,11},{9,8},{10,9... | collective-permute-start | bytes 2359304 | tf_op jit(solution)/shard_map/ppermute | solution.py:246
  122.5 21.3 %collective-permute-start.12 = (bf16[192,2048]{1,0:T(8,128)(2,1)S(1)}, bf16[192,2048]{1,0:T(8,128)(2,1)S(1)}, u32[]{:S(2)}, u32[]{:S(2)}) collective-permute-start(bf16[192,2048]{1,0:T(8,128)(2,1)S(1)} %copy-done.5), channel_id=1, source_target_pairs={{0,1},{1,2},{2,3},{3,0},{4,5},{5,6},{6,7},{7,4},{8,9},{9,10},{10,1... | collective-permute-start | bytes 2359304 | tf_op jit(solution)/shard_map/ppermute | solution.py:246
  124.1 39.3 %all-to-all-start.2 = ((bf16[32,32,256]{2,1,0:T(8,128)(2,1)}), bf16[32,32,256]{2,1,0:T(8,128)(2,1)S(1)}, u32[]{:S(2)}, u32[]{:S(2)}) async-start(bf16[32,32,256]{2,1,0:T(8,128)(2,1)} %bitcast.26), calls=%async_computation.2 | async-start | bytes 1048576 | tf_op jit(solution)/shard_map/all_to_all | solution.py:468
  129.5 18.8 %collective-permute-start.25 = (bf16[192,512]{1,0:T(8,128)(2,1)}, bf16[192,512]{1,0:T(8,128)(2,1)S(1)}, u32[]{:S(2)}, u32[]{:S(2)}) collective-permute-start(bf16[192,512]{1,0:T(8,128)(2,1)} %get-tuple-element.125), channel_id=1, source_target_pairs={{0,1},{1,2},{2,3},{3,0},{4,5},{5,6},{6,7},{7,4},{8,9},{9,10},{10,1... | collective-permute-start | bytes 589832 | tf_op jit(solution)/shard_map/ppermute | solution.py:246
  132.7 21.1 %collective-permute-start.24 = (bf16[192,512]{1,0:T(8,128)(2,1)}, bf16[192,512]{1,0:T(8,128)(2,1)S(1)}, u32[]{:S(2)}, u32[]{:S(2)}) collective-permute-start(bf16[192,512]{1,0:T(8,128)(2,1)} %get-tuple-element.125), channel_id=1, source_target_pairs={{0,2},{1,3},{2,0},{3,1},{4,6},{5,7},{6,4},{7,5},{8,10},{9,11},{10,... | collective-permute-start | bytes 589832 | tf_op jit(solution)/shard_map/ppermute | solution.py:246
  133.4 20.4 %collective-permute-start.23 = (bf16[192,512]{1,0:T(8,128)(2,1)}, bf16[192,512]{1,0:T(8,128)(2,1)S(1)}, u32[]{:S(2)}, u32[]{:S(2)}) collective-permute-start(bf16[192,512]{1,0:T(8,128)(2,1)} %get-tuple-element.125), channel_id=1, source_target_pairs={{0,3},{1,0},{2,1},{3,2},{4,7},{5,4},{6,5},{7,6},{8,11},{9,8},{10,9... | collective-permute-start | bytes 589832 | tf_op jit(solution)/shard_map/ppermute | solution.py:246
  144.2 15.9 %copy-start.9 = (bf16[768,256]{1,0:T(8,128)(2,1)S(1)}, bf16[768,256]{1,0:T(8,128)(2,1)}, u32[]{:S(2)}) copy-start(bf16[768,256]{1,0:T(8,128)(2,1)} %get-tuple-element.106) | copy-start | bytes 1179652
  144.2 15.9 %collective-permute-start.14 = (bf16[96,2048]{1,0:T(8,128)(2,1)S(1)}, bf16[96,2048]{1,0:T(8,128)(2,1)S(1)}, u32[]{:S(2)}, u32[]{:S(2)}) collective-permute-start(bf16[96,2048]{1,0:T(8,128)(2,1)S(1)} %get-tuple-element.86), channel_id=1, source_target_pairs={{0,1},{1,2},{2,3},{3,0},{4,5},{5,6},{6,7},{7,4},{8,9},{9,10},{10,1... | collective-permute-start | bytes 1179656 | tf_op jit(solution)/shard_map/ppermute | solution.py:246
  145.2 14.9 %collective-permute-start.15 = (bf16[96,2048]{1,0:T(8,128)(2,1)S(1)}, bf16[96,2048]{1,0:T(8,128)(2,1)S(1)}, u32[]{:S(2)}, u32[]{:S(2)}) collective-permute-start(bf16[96,2048]{1,0:T(8,128)(2,1)S(1)} %get-tuple-element.87), channel_id=1, source_target_pairs={{0,3},{1,0},{2,1},{3,2},{4,7},{5,4},{6,5},{7,6},{8,11},{9,8},{10,9... | collective-permute-start | bytes 1179656 | tf_op jit(solution)/shard_map/ppermute | solution.py:246
  156.1 6.5 %collective-permute-start.26 = (f32[2,256]{1,0:T(2,128)S(1)}, f32[2,256]{1,0:T(2,128)S(1)}, u32[]{:S(2)}, u32[]{:S(2)}) collective-permute-start(f32[2,256]{1,0:T(2,128)S(1)} %slice.42), channel_id=1, source_target_pairs={{4,0},{8,4},{12,8},{16,12},{20,16},{24,20},{28,24},{32,28},{36,32}... | collective-permute-start | bytes 6152 | tf_op jit(solution)/shard_map/ppermute | solution.py:252
  163.5 13.6 %collective-permute-start.22 = (f32[32,256]{1,0:T(8,128)S(1)}, f32[32,256]{1,0:T(8,128)S(1)}, u32[]{:S(2)}, u32[]{:S(2)}) collective-permute-start(f32[32,256]{1,0:T(8,128)S(1)} %convert_reduce_fusion), channel_id=1, source_target_pairs={{0,0},{1,65},{2,130},{3,195},{4,32},{5,97},{6,162},{7,227},{8,4},{... | collective-permute-start | bytes 98312 | tf_op jit(solution)/shard_map/ppermute | solution.py:484

commit v2 on v1

--- a/solution.py
+++ b/solution.py
@@ -8,6 +8,9 @@
 
 F32 = jnp.float32
 BF16 = jnp.bfloat16
+
+
+STEPS = ((5, 4), (7, 2), (0, 1), (6, 3))
 
 
 def mm(a, b, contract):
@@ -172,9 +175,12 @@
     core = where_ref[1]
     for ref, which in ((sent_ref, 1 - core), (kept_ref, core)):
         columns_t = mid_ref[:, pl.ds(pl.multiple_of(which * side, side), side)].T
+        owned = ref.shape[1]
         for r in range(gated_ref.shape[0]):
-            part = mm(columns_t, gated_ref[r], ((1,), (0,)))
-            ref[r] = part.astype(ref.dtype)
+            part = mm(columns_t, gated_ref[r], ((1,), (0,))).astype(ref.dtype)
+            for k in range(side // owned):
+                z = lax.rem(2 * where_ref[0] + which + STEPS[r][k % 2], 8)
+                ref[z * 4 + k // 2] = part[k * owned : (k + 1) * owned]
 
 
 def down_kernel(member_ref, act, g0, g1, g2, g3a, g3b, out_ref):
@@ -436,13 +442,12 @@
     returned, gated_all = lax.optimization_barrier((returned, gated_all))
 
     core = lax.rem(lax.axis_index("sp"), 2)
-    side = share // 2
     mid_grad, sent, kept = call(
         return_kernel,
         [
             ((tok_rows, share), BF16),
-            ((groups, side, hidden), BF16),
-            ((groups, side, hidden), F32),
+            ((sources // 2, width // sources, hidden), BF16),
+            ((sources // 2, width // sources, hidden), F32),
         ],
         [
             pltpu.VMEM((experts * packed, 128), F32),
@@ -464,9 +469,8 @@
 
     paired = (kept + swapped.astype(F32)).astype(BF16)
     chips = sources // 2
-    owned = width // sources
     pieces = lax.all_to_all(
-        paired.reshape(chips, owned, hidden),
+        paired,
         "sp",
         0,
         0,
@@ -474,13 +478,16 @@
         tiled=True,
     )
     out_weight_sum = jnp.sum(pieces.astype(F32), axis=0)
-    per = chips // groups
     pairs = []
-    for j in range(chips):
-        for c in range(2):
-            for m in range(groups):
-                s = (sources // groups) * m + per * c + j % per
-                pairs.append(((2 * j + c) * groups + m, s * groups + (m + j // per) % groups))
+    for z in range(8):
+        for y in range(4):
+            for c in range(2):
+                for m in range(groups):
+                    step = (z - 2 * m - c) % 8
+                    r, k = next((r, k) for r in range(4) for k in range(2) if STEPS[r][k] == step)
+                    here = (z * 4 + y) * 2 + c
+                    owner = 16 * m + 8 * c + 2 * y + k
+                    pairs.append((here * groups + m, owner * groups + (m + r) % groups))
     out_weight_grad = lax.ppermute(out_weight_sum, ("sp", "tp"), pairs)
 
     mid_rel = jnp.concatenate([mid_grad, mid_right, mid_far, mid_left], axis=1)

time: 178 us -> 175 us (0.983)
  the two profiles are of different devices: /device:TPU:20 before, /device:TPU:1 now
where the time goes in v2:
time: 175 us; the launch traced here: 174 us
  starting transfers between devices  72.5 us (41%)
  waiting for transfers between devices  61.8 us (35%)
  Pallas kernels  24.1 us (14%)
  other arithmetic  6.67 us (4%)
  matrix products  5.52 us (3%)
  local copies, waits for them, and re-layouts  2.94 us (2%)
    ppermute x23, waiting for transfers between devices, turn(): lax.ppermute(shard, 'tp', [(i, (i + by) % peers) for i in range(peers)])  36.3 us
    ppermute x23, starting transfers between devices, turn(): lax.ppermute(shard, 'tp', [(i, (i + by) % peers) for i in range(peers)])  29.5 us
    pallas_call x10, Pallas kernels, call(): pl.pallas_call(kernel, out_shape=[jax.ShapeDtypeStruct(*o) for o in outs]...  20.4 us
    all_to_all x1, waiting for transfers between devices, on_device(): lax.all_to_all(leaving.reshape(sources, packed, 128), 'sp', split_axis=0,...  15.3 us
    ppermute x2, starting transfers between devices, passed_along(): return lax.ppermute(shard, axis, pairs)  13.4 us
    all_to_all x1, starting transfers between devices, on_device(): lax.all_to_all(piece.reshape(experts, packed, 128), 'sp', split_axis=0, c...  12.9 us
    all_to_all x1, starting transfers between devices, on_device(): lax.all_to_all(leaving.reshape(sources, packed, 128), 'sp', split_axis=0,...  9.55 us
    dot_general x3, matrix products, mm(): lax.dot_general(a, b, ((contract[0], contract[1]), ((), ())), preferred_e...  5.52 us
  transfers between devices with their start and end apart: 30, of which 16 were waited for; matrix products, arithmetic and copies ran while one was open for 7% of the time, Pallas kernels for 11%

profile of v2, /device:TPU:1, one launch (start us, length us, event | category | flops | bytes accessed | tf_op | source)
XLA Modules:
  0.0 174.4 jit_solution(5253598509324498102)
XLA Ops:
  0.6 3.4 %collective-permute-start.1 = (bf16[256,2048]{1,0:T(8,128)(2,1)}, bf16[256,2048]{1,0:T(8,128)(2,1)}, u32[]{:S(2)}, u32[]{:S(2)}) collective-permute-start(bf16[256,2048]{1,0:T(8,128)(2,1)} %bitcast.50), channel_id=1, source_target_pairs={{0,3},{1,0},{2,1},{3,2},{4,7},{5,4},{6,5},{7,6},{8,11},{9,8},{10,9... | collective-permute-start | bytes 3145736 | tf_op jit(solution)/shard_map/ppermute | solution.py:252
  4.0 2.8 %shard_map.179 = bf16[3072,128]{1,0:T(8,128)(2,1)} custom-call(s32[1]{0:T(128)} %bitcast.1.first_ref, s32[2,192]{1,0:T(2,128)} %bitcast.46, f32[2,192]{1,0:T(2,128)} %bitcast.63, bf16[192,2048]{1,0:T(8,128)(2,1)} %tokens_hbm.3), custom_call_target="tpu_custom_call" | custom-call | tf_op jit(solution)/shard_map/pallas_call | solution.py:240
  6.8 12.9 %all-to-all-start = ((bf16[64,48,128]{2,1,0:T(8,128)(2,1)}), bf16[64,48,128]{2,1,0:T(8,128)(2,1)}, u32[]{:S(2)}, u32[]{:S(2)}) async-start(bf16[64,48,128]{2,1,0:T(8,128)(2,1)} %bitcast.48), calls=%async_computation | async-start | bytes 1572864 | tf_op jit(solution)/shard_map/all_to_all | solution.py:328
  19.8 3.8 %fusion = bf16[2048,256]{1,0:T(8,128)(2,1)} fusion(s32[]{:T(128)S(6)} %select_n.3, bf16[2048,256]{1,0:T(8,128)(2,1)S(1)} %copy-done.12), kind=kLoop, calls=%fused_computation.2 | loop fusion | flops 2097152 | bytes 2097156 | tf_op jit(solution)/shard_map/concatenate | solution.py:333
  23.6 2.6 %collective-permute-done.1.right.w2_hbm = bf16[256,2048]{1,0:T(8,128)(2,1)} collective-permute-done((bf16[256,2048]{1,0:T(8,128)(2,1)}, bf16[256,2048]{1,0:T(8,128)(2,1)}, u32[]{:S(2)}, u32[]{:S(2)}) %collective-permute-start.1) | collective-permute-done | bytes 1048608 | tf_op jit(solution)/shard_map/ppermute | solution.py:252
  26.2 3.1 %collective-permute-done.left.w1_hbm = bf16[256,2048]{1,0:T(8,128)(2,1)} collective-permute-done((bf16[256,2048]{1,0:T(8,128)(2,1)}, bf16[256,2048]{1,0:T(8,128)(2,1)}, u32[]{:S(2)}, u32[]{:S(2)}) %collective-permute-start) | collective-permute-done | bytes 1048608 | tf_op jit(solution)/shard_map/ppermute | solution.py:252
  29.3 2.2 %shard_map.180 = (bf16[128,2048]{1,0:T(8,128)(2,1)}, bf16[128,2048]{1,0:T(8,128)(2,1)}) custom-call(bf16[256,2048]{1,0:T(8,128)(2,1)} %collective-permute-done.left.w1_hbm, bf16[256,2048]{1,0:T(8,128)(2,1)} %collective-permute-done.1.right.w2_hbm), custom_call_target="tpu_custom_call" | custom-call | tf_op jit(solution)/shard_map/pallas_call | solution.py:240
  31.6 2.7 %collective-permute-start.4 = (bf16[128,2048]{1,0:T(8,128)(2,1)}, bf16[128,2048]{1,0:T(8,128)(2,1)}, u32[]{:S(2)}, u32[]{:S(2)}) collective-permute-start(bf16[128,2048]{1,0:T(8,128)(2,1)} %get-tuple-element.59), channel_id=1, source_target_pairs={{0,3},{1,0},{2,1},{3,2},{4,7},{5,4},{6,5},{7,6},{8,11},{9,8},{10,9... | collective-permute-start | bytes 1572872 | tf_op jit(solution)/shard_map/ppermute | solution.py:252
  34.3 1.0 fusion.26
  35.5 2.2 %multiply_convert_fusion = (bf16[768,256]{1,0:T(8,128)(2,1)}, f32[768,256]{1,0:T(8,128)S(1)}, f32[768,256]{1,0:T(8,128)}) fusion(f32[768,256]{1,0:T(8,128)S(1)} %fusion.26, bf16[768,2048]{1,0:T(8,128)(2,1)S(1)} %bitcast.43, bf16[1,2048,256]{2,1,0:T(8,128)(2,1)S(1)} %copy-done.1), kind=kOutput, calls=%fused_computation.15 | convolution fusion | flops 807469056 | bytes 6946816 | tf_op jit(solution)/shard_map/dot_general | solution.py:17
  37.7 5.0 %all-to-all-done = bf16[64,48,128]{2,1,0:T(8,128)(2,1)} async-done(((bf16[64,48,128]{2,1,0:T(8,128)(2,1)}), bf16[64,48,128]{2,1,0:T(8,128)(2,1)}, u32[]{:S(2)}, u32[]{:S(2)}) %all-to-all-start) | async-done | bytes 786464 | tf_op jit(solution)/shard_map/all_to_all | solution.py:328
  42.7 4.4 %shard_map.181 = (bf16[192,2048]{1,0:T(8,128)(2,1)}, bf16[192,256]{1,0:T(8,128)(2,1)}, bf16[192,256]{1,0:T(8,128)(2,1)}, bf16[192,256]{1,0:T(8,128)(2,1)}) custom-call(bf16[3072,128]{1,0:T(8,128)(2,1)} %bitcast.12.arrived_hbm, bf16[256,2048]{1,0:T(8,128)(2,1)} %bitcast.52, bf16[256,2048]{1,0:T(8,128)(2,1)} %collective-permute-done.left.w1_hbm, ...), custom_call_target="tpu_custom_call" | custom-call | tf_op jit(solution)/shard_map/pallas_call | solution.py:240
  47.1 3.2 %collective-permute-start.2 = (bf16[192,256]{1,0:T(8,128)(2,1)}, bf16[192,256]{1,0:T(8,128)(2,1)S(1)}, u32[]{:S(2)}, u32[]{:S(2)}) collective-permute-start(bf16[192,256]{1,0:T(8,128)(2,1)} %get-tuple-element.64), channel_id=1, source_target_pairs={{0,3},{1,0},{2,1},{3,2},{4,7},{5,4},{6,5},{7,6},{8,11},{9,8},{10,9... | collective-permute-start | bytes 294920 | tf_op jit(solution)/shard_map/ppermute | solution.py:252
  50.3 1.1 copy-done.4
  51.4 1.8 %shard_map.182 = bf16[192,256]{1,0:T(8,128)(2,1)S(1)} custom-call(bf16[192,2048]{1,0:T(8,128)(2,1)S(1)} %copy-done.4, bf16[128,2048]{1,0:T(8,128)(2,1)} %collective-permute-done.3.w3a, bf16[128,2048]{1,0:T(8,128)(2,1)} %collective-permute-done.4.w3b), custom_call_target="tpu_custom_call" | custom-call | tf_op jit(solution)/shard_map/pallas_call | solution.py:240
  53.3 1.4 collective-permute-start.5
  55.2 3.2 %collective-permute-done.5.far = bf16[192,256]{1,0:T(8,128)(2,1)S(1)} collective-permute-done((bf16[192,256]{1,0:T(8,128)(2,1)S(1)}, bf16[192,256]{1,0:T(8,128)(2,1)S(1)}, u32[]{:S(2)}, u32[]{:S(2)}) %collective-permute-start.5) | collective-permute-done | bytes 98336 | tf_op jit(solution)/shard_map/ppermute | solution.py:252
  58.3 0.9 copy-done.10
  59.9 2.7 %collective-permute-start.9 = (bf16[384,512]{1,0:T(8,128)(2,1)S(1)}, bf16[384,512]{1,0:T(8,128)(2,1)S(1)}, u32[]{:S(2)}, u32[]{:S(2)}) collective-permute-start(bf16[384,512]{1,0:T(8,128)(2,1)S(1)} %get-tuple-element.74), channel_id=1, source_target_pairs={{0,3},{1,0},{2,1},{3,2},{4,7},{5,4},{6,5},{7,6},{8,11},{9,8},{10,9... | collective-permute-start | bytes 1179656 | tf_op jit(solution)/shard_map/ppermute | solution.py:252
  62.7 1.4 shard_map.184
  64.1 2.7 %collective-permute-start.16 = (bf16[384,512]{1,0:T(8,128)(2,1)S(1)}, bf16[384,512]{1,0:T(8,128)(2,1)S(1)}, u32[]{:S(2)}, u32[]{:S(2)}) collective-permute-start(bf16[384,512]{1,0:T(8,128)(2,1)S(1)} %get-tuple-element.90), channel_id=1, source_target_pairs={{0,3},{1,0},{2,1},{3,2},{4,7},{5,4},{6,5},{7,6},{8,11},{9,8},{10,9... | collective-permute-start | bytes 1179656 | tf_op jit(solution)/shard_map/ppermute | solution.py:252
  66.8 1.9 %collective-permute-done.9 = bf16[384,512]{1,0:T(8,128)(2,1)S(1)} collective-permute-done((bf16[384,512]{1,0:T(8,128)(2,1)S(1)}, bf16[384,512]{1,0:T(8,128)(2,1)S(1)}, u32[]{:S(2)}, u32[]{:S(2)}) %collective-permute-start.9) | collective-permute-done | bytes 393248 | tf_op jit(solution)/shard_map/ppermute | solution.py:252
  68.8 3.5 %collective-permute-start.10 = (bf16[384,512]{1,0:T(8,128)(2,1)S(1)}, bf16[384,512]{1,0:T(8,128)(2,1)S(1)}, u32[]{:S(2)}, u32[]{:S(2)}) collective-permute-start(bf16[384,512]{1,0:T(8,128)(2,1)S(1)} %add_convert_fusion.1), channel_id=1, source_target_pairs={{0,3},{1,0},{2,1},{3,2},{4,7},{5,4},{6,5},{7,6},{8,11},{9,8},{10,9... | collective-permute-start | bytes 1179656 | tf_op jit(solution)/shard_map/ppermute | solution.py:252
  72.6 9.4 %collective-permute-start.11 = (f32[2,256]{1,0:T(2,128)S(1)}, f32[2,256]{1,0:T(2,128)S(1)}, u32[]{:S(2)}, u32[]{:S(2)}) collective-permute-start(f32[2,256]{1,0:T(2,128)S(1)} %slice.39), channel_id=1, source_target_pairs={{0,4},{4,8},{8,12},{12,16},{16,20},{20,24},{24,28},{28,32},{32,36}... | collective-permute-start | bytes 6152 | tf_op jit(solution)/shard_map/ppermute | solution.py:258
  82.0 3.6 %weights.1 = (bf16[2048,256]{1,0:T(8,128)(2,1)}, bf16[2048,256]{1,0:T(8,128)(2,1)}) custom-call(bf16[768,2048]{1,0:T(8,128)(2,1)S(1)} %bitcast.44, bf16[768,256]{1,0:T(8,128)(2,1)S(1)} %get-tuple-element.69.gate_part, bf16[768,256]{1,0:T(8,128)(2,1)S(1)} %get-tuple-element.70.up_part), custom_call_target="tpu_custom_call" | custom-call | tf_op jit(solution)/shard_map/weights/pallas_call | solution.py:225
  85.7 3.0 %collective-permute-done.8.left_a = bf16[384,512]{1,0:T(8,128)(2,1)S(1)} collective-permute-done((bf16[384,512]{1,0:T(8,128)(2,1)S(1)}, bf16[384,512]{1,0:T(8,128)(2,1)S(1)}, u32[]{:S(2)}, u32[]{:S(2)}) %collective-permute-start.8) | collective-permute-done | bytes 393248 | tf_op jit(solution)/shard_map/ppermute | solution.py:252
  88.7 1.5 shard_map.187
  90.2 9.6 %all-to-all-start.1 = ((bf16[64,48,128]{2,1,0:T(8,128)(2,1)}), bf16[64,48,128]{2,1,0:T(8,128)(2,1)S(1)}, u32[]{:S(2)}, u32[]{:S(2)}) async-start(bf16[64,48,128]{2,1,0:T(8,128)(2,1)} %bitcast.20), calls=%async_computation.1 | async-start | bytes 1572864 | tf_op jit(solution)/shard_map/all_to_all | solution.py:431
  99.9 1.2 collective-permute-start.19
  101.1 1.5 collective-permute-start.18
  102.6 4.7 %collective-permute-done.20 = bf16[192,256]{1,0:T(8,128)(2,1)S(1)} collective-permute-done((bf16[192,256]{1,0:T(8,128)(2,1)S(1)}, bf16[192,256]{1,0:T(8,128)(2,1)S(1)}, u32[]{:S(2)}, u32[]{:S(2)}) %collective-permute-start.20) | collective-permute-done | bytes 98336 | tf_op jit(solution)/shard_map/ppermute | solution.py:252
  107.5 15.3 %all-to-all-done.1 = bf16[64,48,128]{2,1,0:T(8,128)(2,1)S(1)} async-done(((bf16[64,48,128]{2,1,0:T(8,128)(2,1)}), bf16[64,48,128]{2,1,0:T(8,128)(2,1)S(1)}, u32[]{:S(2)}, u32[]{:S(2)}) %all-to-all-start.1) | async-done | bytes 786464 | tf_op jit(solution)/shard_map/all_to_all | solution.py:431
  122.8 2.7 %shard_map.188 = (bf16[192,512]{1,0:T(8,128)(2,1)}, bf16[32,32,256]{2,1,0:T(8,128)(2,1)S(1)}, f32[32,32,256]{2,1,0:T(8,128)S(1)}) custom-call(s32[2]{0:T(128)S(1)} %pad_add_fusion.where_ref, s32[2,192]{1,0:T(2,128)S(1)} %bitcast.47, bf16[3072,128]{1,0:T(8,128)(2,1)S(1)} %bitcast.41, bf16[192,2048]{1,0:T(8,128)(2,1)S(1)} %copy-done.3, ...), custom_call_target="tpu_custom_call" | custom-call | tf_op jit(solution)/shard_map/pallas_call | solution.py:240
  125.5 0.8 collective-permute-start.21
  126.3 1.5 collective-permute-start.12
  127.8 1.0 add_convert_fusion
  128.8 4.8 %all-to-all-start.2 = ((bf16[32,32,256]{2,1,0:T(8,128)(2,1)}), bf16[32,32,256]{2,1,0:T(8,128)(2,1)S(1)}, u32[]{:S(2)}, u32[]{:S(2)}) async-start(bf16[32,32,256]{2,1,0:T(8,128)(2,1)} %add_convert_fusion), calls=%async_computation.2 | async-start | bytes 1048576 | tf_op jit(solution)/shard_map/all_to_all | solution.py:472
  133.7 2.3 %collective-permute-start.24 = (bf16[192,512]{1,0:T(8,128)(2,1)}, bf16[192,512]{1,0:T(8,128)(2,1)S(1)}, u32[]{:S(2)}, u32[]{:S(2)}) collective-permute-start(bf16[192,512]{1,0:T(8,128)(2,1)} %get-tuple-element.125), channel_id=1, source_target_pairs={{0,2},{1,3},{2,0},{3,1},{4,6},{5,7},{6,4},{7,5},{8,10},{9,11},{10,... | collective-permute-start | bytes 589832 | tf_op jit(solution)/shard_map/ppermute | solution.py:252
  136.4 9.0 %collective-permute-done.13.right.g2 = bf16[192,2048]{1,0:T(8,128)(2,1)S(1)} collective-permute-done((bf16[192,2048]{1,0:T(8,128)(2,1)S(1)}, bf16[192,2048]{1,0:T(8,128)(2,1)S(1)}, u32[]{:S(2)}, u32[]{:S(2)}) %collective-permute-start.13) | collective-permute-done | bytes 786464 | tf_op jit(solution)/shard_map/ppermute | solution.py:252
  145.3 0.9 collective-permute-done.12.left.g1
  147.0 2.4 %collective-permute-start.15 = (bf16[96,2048]{1,0:T(8,128)(2,1)S(1)}, bf16[96,2048]{1,0:T(8,128)(2,1)S(1)}, u32[]{:S(2)}, u32[]{:S(2)}) collective-permute-start(bf16[96,2048]{1,0:T(8,128)(2,1)S(1)} %get-tuple-element.87), channel_id=1, source_target_pairs={{0,3},{1,0},{2,1},{3,2},{4,7},{5,4},{6,5},{7,6},{8,11},{9,8},{10,9... | collective-permute-start | bytes 1179656 | tf_op jit(solution)/shard_map/ppermute | solution.py:252
  149.4 5.2 %collective-permute-done.25 = bf16[192,512]{1,0:T(8,128)(2,1)S(1)} collective-permute-done((bf16[192,512]{1,0:T(8,128)(2,1)}, bf16[192,512]{1,0:T(8,128)(2,1)S(1)}, u32[]{:S(2)}, u32[]{:S(2)}) %collective-permute-start.25) | collective-permute-done | bytes 196640 | tf_op jit(solution)/shard_map/ppermute | solution.py:252
  154.6 2.4 %multiply_convert_fusion.1 = (bf16[192,256]{1,0:T(8,128)(2,1)}, f32[192,256]{1,0:T(8,128)S(1)}) fusion(f32[192,256]{1,0:T(8,128)S(1)} %get-tuple-element.101, bf16[192,256]{1,0:T(8,128)(2,1)S(1)} %copy-done.15, bf16[2048,256]{1,0:T(8,128)(2,1)} %fusion, bf16[192,512]{1,0:T(8,128)(2,1)S(1)} %collective-permute-done.25, ...), kind=kOutput, calls=%fused_computation.44 | convolution fusion | flops 204668928 | bytes 2424832 | tf_op jit(solution)/shard_map/dot_general | solution.py:17
  157.0 4.0 %collective-permute-start.26 = (f32[2,256]{1,0:T(2,128)S(1)}, f32[2,256]{1,0:T(2,128)S(1)}, u32[]{:S(2)}, u32[]{:S(2)}) collective-permute-start(f32[2,256]{1,0:T(2,128)S(1)} %slice.42), channel_id=1, source_target_pairs={{4,0},{8,4},{12,8},{16,12},{20,16},{24,20},{28,24},{32,28},{36,32}... | collective-permute-start | bytes 6152 | tf_op jit(solution)/shard_map/ppermute | solution.py:258
  161.0 2.1 %collective-permute-done.14.g3a = bf16[96,2048]{1,0:T(8,128)(2,1)S(1)} collective-permute-done((bf16[96,2048]{1,0:T(8,128)(2,1)S(1)}, bf16[96,2048]{1,0:T(8,128)(2,1)S(1)}, u32[]{:S(2)}, u32[]{:S(2)}) %collective-permute-start.14) | collective-permute-done | bytes 393248 | tf_op jit(solution)/shard_map/ppermute | solution.py:252
  163.1 2.5 %shard_map.186 = bf16[256,2048]{1,0:T(8,128)(2,1)} custom-call(s32[1]{0:T(128)} %bitcast.member_ref, bf16[4,192,256]{2,1,0:T(8,128)(2,1)S(1)} %bitcast.45, bf16[192,2048]{1,0:T(8,128)(2,1)S(1)} %copy-done.5, bf16[192,2048]{1,0:T(8,128)(2,1)S(1)} %collective-permute-done.12.left.g1, bf16[192,2048]{1,0:T(8,128)(2,1)S(1)} %collective-permute-done.13.right.g2, ...), custom_call_target="tpu_custom_call" | custom-call | tf_op jit(solution)/shard_map/pallas_call | solution.py:240
  166.4 1.6 collective-permute-start.22
  168.7 5.1 %collective-permute-done.22 = f32[32,256]{1,0:T(8,128)S(1)} collective-permute-done((f32[32,256]{1,0:T(8,128)S(1)}, f32[32,256]{1,0:T(8,128)S(1)}, u32[]{:S(2)}, u32[]{:S(2)}) %collective-permute-start.22) | collective-permute-done | bytes 32800 | tf_op jit(solution)/shard_map/ppermute | solution.py:491
  (75 shorter events, 5.7 us)
Async XLA Ops:
  0.6 25.5 %collective-permute-start.1 = (bf16[256,2048]{1,0:T(8,128)(2,1)}, bf16[256,2048]{1,0:T(8,128)(2,1)}, u32[]{:S(2)}, u32[]{:S(2)}) collective-permute-start(bf16[256,2048]{1,0:T(8,128)(2,1)} %bitcast.50), channel_id=1, source_target_pairs={{0,3},{1,0},{2,1},{3,2},{4,7},{5,4},{6,5},{7,6},{8,11},{9,8},{10,9... | collective-permute-start | bytes 3145736 | tf_op jit(solution)/shard_map/ppermute | solution.py:252
  4.0 25.3 %collective-permute-start = (bf16[256,2048]{1,0:T(8,128)(2,1)}, bf16[256,2048]{1,0:T(8,128)(2,1)}, u32[]{:S(2)}, u32[]{:S(2)}) collective-permute-start(bf16[256,2048]{1,0:T(8,128)(2,1)} %bitcast.51), channel_id=1, source_target_pairs={{0,1},{1,2},{2,3},{3,0},{4,5},{5,6},{6,7},{7,4},{8,9},{9,10},{10,1... | collective-permute-start | bytes 3145736 | tf_op jit(solution)/shard_map/ppermute | solution.py:252
  6.8 12.9 %copy-start.12 = (bf16[2048,256]{1,0:T(8,128)(2,1)S(1)}, bf16[2048,256]{1,0:T(8,128)(2,1)}, u32[]{:S(2)}) copy-start(bf16[2048,256]{1,0:T(8,128)(2,1)} %param.23) | copy-start | bytes 3145732
  6.8 35.9 %all-to-all-start = ((bf16[64,48,128]{2,1,0:T(8,128)(2,1)}), bf16[64,48,128]{2,1,0:T(8,128)(2,1)}, u32[]{:S(2)}, u32[]{:S(2)}) async-start(bf16[64,48,128]{2,1,0:T(8,128)(2,1)} %bitcast.48), calls=%async_computation | async-start | bytes 1572864 | tf_op jit(solution)/shard_map/all_to_all | solution.py:328
  19.7 14.5 %copy-start = (bf16[1,2048,256]{2,1,0:T(8,128)(2,1)S(1)}, bf16[1,2048,256]{2,1,0:T(8,128)(2,1)}, u32[]{:S(2)}) copy-start(bf16[1,2048,256]{2,1,0:T(8,128)(2,1)} %param.16) | copy-start | bytes 3145732
  19.7 14.5 %copy-start.6 = (bf16[64,1,12,2048]{3,0,2,1:T(8,128)(2,1)S(1)}, bf16[64,1,12,2048]{3,0,2,1:T(8,128)(2,1)}, u32[]{:S(2)}) copy-start(bf16[64,1,12,2048]{3,0,2,1:T(8,128)(2,1)} %param.15) | copy-start | bytes 9437188
  31.5 18.8 %collective-permute-start.3 = (bf16[128,2048]{1,0:T(8,128)(2,1)}, bf16[128,2048]{1,0:T(8,128)(2,1)}, u32[]{:S(2)}, u32[]{:S(2)}) collective-permute-start(bf16[128,2048]{1,0:T(8,128)(2,1)} %get-tuple-element.58), channel_id=1, source_target_pairs={{0,1},{1,2},{2,3},{3,0},{4,5},{5,6},{6,7},{7,4},{8,9},{9,10},{10,1... | collective-permute-start | bytes 1572872 | tf_op jit(solution)/shard_map/ppermute | solution.py:252
  31.6 18.7 %collective-permute-start.4 = (bf16[128,2048]{1,0:T(8,128)(2,1)}, bf16[128,2048]{1,0:T(8,128)(2,1)}, u32[]{:S(2)}, u32[]{:S(2)}) collective-permute-start(bf16[128,2048]{1,0:T(8,128)(2,1)} %get-tuple-element.59), channel_id=1, source_target_pairs={{0,3},{1,0},{2,1},{3,2},{4,7},{5,4},{6,5},{7,6},{8,11},{9,8},{10,9... | collective-permute-start | bytes 1572872 | tf_op jit(solution)/shard_map/ppermute | solution.py:252
  34.3 1.2 copy-start.1
  47.1 11.3 %copy-start.2 = (bf16[1,2048,256]{2,1,0:T(8,128)(2,1)S(1)}, bf16[1,2048,256]{2,1,0:T(8,128)(2,1)}, u32[]{:S(2)}) copy-start(bf16[1,2048,256]{2,1,0:T(8,128)(2,1)} %param.17) | copy-start | bytes 3145732
  47.1 7.6 %collective-permute-start.2 = (bf16[192,256]{1,0:T(8,128)(2,1)}, bf16[192,256]{1,0:T(8,128)(2,1)S(1)}, u32[]{:S(2)}, u32[]{:S(2)}) collective-permute-start(bf16[192,256]{1,0:T(8,128)(2,1)} %get-tuple-element.64), channel_id=1, source_target_pairs={{0,3},{1,0},{2,1},{3,2},{4,7},{5,4},{6,5},{7,6},{8,11},{9,8},{10,9... | collective-permute-start | bytes 294920 | tf_op jit(solution)/shard_map/ppermute | solution.py:252
  50.3 4.9 %collective-permute-start.6 = (bf16[192,256]{1,0:T(8,128)(2,1)}, bf16[192,256]{1,0:T(8,128)(2,1)S(1)}, u32[]{:S(2)}, u32[]{:S(2)}) collective-permute-start(bf16[192,256]{1,0:T(8,128)(2,1)} %get-tuple-element.66), channel_id=1, source_target_pairs={{0,1},{1,2},{2,3},{3,0},{4,5},{5,6},{6,7},{7,4},{8,9},{9,10},{10,1... | collective-permute-start | bytes 294920 | tf_op jit(solution)/shard_map/ppermute | solution.py:252
  50.3 1.1 copy-start.4
  51.4 6.9 %copy-start.8 = (f32[768,256]{1,0:T(8,128)S(1)}, f32[768,256]{1,0:T(8,128)}, u32[]{:S(2)}) copy-start(f32[768,256]{1,0:T(8,128)} %get-tuple-element.67.up_of) | copy-start | bytes 2359300
  53.3 5.1 %collective-permute-start.5 = (bf16[192,256]{1,0:T(8,128)(2,1)S(1)}, bf16[192,256]{1,0:T(8,128)(2,1)S(1)}, u32[]{:S(2)}, u32[]{:S(2)}) collective-permute-start(bf16[192,256]{1,0:T(8,128)(2,1)S(1)} %shard_map.182), channel_id=1, source_target_pairs={{0,2},{1,3},{2,0},{3,1},{4,6},{5,7},{6,4},{7,5},{8,10},{9,11},{10,... | collective-permute-start | bytes 294920 | tf_op jit(solution)/shard_map/ppermute | solution.py:252
  58.3 0.9 copy-start.10
  59.9 8.8 %collective-permute-start.9 = (bf16[384,512]{1,0:T(8,128)(2,1)S(1)}, bf16[384,512]{1,0:T(8,128)(2,1)S(1)}, u32[]{:S(2)}, u32[]{:S(2)}) collective-permute-start(bf16[384,512]{1,0:T(8,128)(2,1)S(1)} %get-tuple-element.74), channel_id=1, source_target_pairs={{0,3},{1,0},{2,1},{3,2},{4,7},{5,4},{6,5},{7,6},{8,11},{9,8},{10,9... | collective-permute-start | bytes 1179656 | tf_op jit(solution)/shard_map/ppermute | solution.py:252
  62.7 9.7 %collective-permute-start.7 = (bf16[384,512]{1,0:T(8,128)(2,1)S(1)}, bf16[384,512]{1,0:T(8,128)(2,1)S(1)}, u32[]{:S(2)}, u32[]{:S(2)}) collective-permute-start(bf16[384,512]{1,0:T(8,128)(2,1)S(1)} %get-tuple-element.72), channel_id=1, source_target_pairs={{0,1},{1,2},{2,3},{3,0},{4,5},{5,6},{6,7},{7,4},{8,9},{9,10},{10,1... | collective-permute-start | bytes 1179656 | tf_op jit(solution)/shard_map/ppermute | solution.py:252
  62.7 9.9 %copy-start.13 = (bf16[192,256]{1,0:T(8,128)(2,1)S(1)}, bf16[192,256]{1,0:T(8,128)(2,1)}, u32[]{:S(2)}) copy-start(bf16[192,256]{1,0:T(8,128)(2,1)} %param.19) | copy-start | bytes 294916
  62.7 9.9 %copy-start.14 = (bf16[192,256]{1,0:T(8,128)(2,1)S(1)}, bf16[192,256]{1,0:T(8,128)(2,1)}, u32[]{:S(2)}) copy-start(bf16[192,256]{1,0:T(8,128)(2,1)} %param.21) | copy-start | bytes 294916
  62.7 19.4 %copy-start.7 = (bf16[64,1,12,2048]{3,0,2,1:T(8,128)(2,1)S(1)}, bf16[64,1,12,2048]{3,0,2,1:T(8,128)(2,1)}, u32[]{:S(2)}) copy-start(bf16[64,1,12,2048]{3,0,2,1:T(8,128)(2,1)} %param.15) | copy-start | bytes 9437188
  64.1 17.9 %copy-start.16 = (f32[3,256]{1,0:T(4,128)S(1)}, f32[3,256]{1,0:T(4,128)}, u32[]{:S(2)}) copy-start(f32[3,256]{1,0:T(4,128)} %param.22) | copy-start | bytes 9220
  64.1 24.6 %collective-permute-start.16 = (bf16[384,512]{1,0:T(8,128)(2,1)S(1)}, bf16[384,512]{1,0:T(8,128)(2,1)S(1)}, u32[]{:S(2)}, u32[]{:S(2)}) collective-permute-start(bf16[384,512]{1,0:T(8,128)(2,1)S(1)} %get-tuple-element.90), channel_id=1, source_target_pairs={{0,3},{1,0},{2,1},{3,2},{4,7},{5,4},{6,5},{7,6},{8,11},{9,8},{10,9... | collective-permute-start | bytes 1179656 | tf_op jit(solution)/shard_map/ppermute | solution.py:252
  66.8 21.9 %collective-permute-start.17 = (bf16[384,512]{1,0:T(8,128)(2,1)S(1)}, bf16[384,512]{1,0:T(8,128)(2,1)S(1)}, u32[]{:S(2)}, u32[]{:S(2)}) collective-permute-start(bf16[384,512]{1,0:T(8,128)(2,1)S(1)} %get-tuple-element.91), channel_id=1, source_target_pairs={{0,1},{1,2},{2,3},{3,0},{4,5},{5,6},{6,7},{7,4},{8,9},{9,10},{10,1... | collective-permute-start | bytes 1179656 | tf_op jit(solution)/shard_map/ppermute | solution.py:252
  68.8 16.9 %collective-permute-start.10 = (bf16[384,512]{1,0:T(8,128)(2,1)S(1)}, bf16[384,512]{1,0:T(8,128)(2,1)S(1)}, u32[]{:S(2)}, u32[]{:S(2)}) collective-permute-start(bf16[384,512]{1,0:T(8,128)(2,1)S(1)} %add_convert_fusion.1), channel_id=1, source_target_pairs={{0,3},{1,0},{2,1},{3,2},{4,7},{5,4},{6,5},{7,6},{8,11},{9,8},{10,9... | collective-permute-start | bytes 1179656 | tf_op jit(solution)/shard_map/ppermute | solution.py:252
  72.4 13.2 %copy-start.15 = (bf16[192,256]{1,0:T(8,128)(2,1)S(1)}, bf16[192,256]{1,0:T(8,128)(2,1)}, u32[]{:S(2)}) copy-start(bf16[192,256]{1,0:T(8,128)(2,1)} %param.20) | copy-start | bytes 294916
  72.4 16.3 %collective-permute-start.8 = (bf16[384,512]{1,0:T(8,128)(2,1)S(1)}, bf16[384,512]{1,0:T(8,128)(2,1)S(1)}, u32[]{:S(2)}, u32[]{:S(2)}) collective-permute-start(bf16[384,512]{1,0:T(8,128)(2,1)S(1)} %add_convert_fusion.2), channel_id=1, source_target_pairs={{0,1},{1,2},{2,3},{3,0},{4,5},{5,6},{6,7},{7,4},{8,9},{9,10},{10,1... | collective-permute-start | bytes 1179656 | tf_op jit(solution)/shard_map/ppermute | solution.py:252
  72.6 13.1 %collective-permute-start.11 = (f32[2,256]{1,0:T(2,128)S(1)}, f32[2,256]{1,0:T(2,128)S(1)}, u32[]{:S(2)}, u32[]{:S(2)}) collective-permute-start(f32[2,256]{1,0:T(2,128)S(1)} %slice.39), channel_id=1, source_target_pairs={{0,4},{4,8},{8,12},{12,16},{16,20},{20,24},{24,28},{28,32},{32,36}... | collective-permute-start | bytes 6152 | tf_op jit(solution)/shard_map/ppermute | solution.py:258
  90.2 32.6 %copy-start.3 = (bf16[192,2048]{1,0:T(8,128)(2,1)S(1)}, bf16[192,2048]{1,0:T(8,128)(2,1)}, u32[]{:S(2)}) copy-start(bf16[192,2048]{1,0:T(8,128)(2,1)} %tokens_hbm.3) | copy-start | bytes 2359300
  90.2 32.6 %copy-start.11 = (s32[192,2]{0,1:T(2,128)S(1)}, s32[192,2]{0,1:T(2,128)}, u32[]{:S(2)}) copy-start(s32[192,2]{0,1:T(2,128)} %param.13) | copy-start | bytes 4612
  90.2 36.1 %copy-start.5 = (bf16[192,2048]{1,0:T(8,128)(2,1)S(1)}, bf16[192,2048]{1,0:T(8,128)(2,1)}, u32[]{:S(2)}) copy-start(bf16[192,2048]{1,0:T(8,128)(2,1)} %get-tuple-element.83.rows_ref.g0) | copy-start | bytes 2359300
  90.2 32.6 %all-to-all-start.1 = ((bf16[64,48,128]{2,1,0:T(8,128)(2,1)}), bf16[64,48,128]{2,1,0:T(8,128)(2,1)S(1)}, u32[]{:S(2)}, u32[]{:S(2)}) async-start(bf16[64,48,128]{2,1,0:T(8,128)(2,1)} %bitcast.20), calls=%async_computation.1 | async-start | bytes 1572864 | tf_op jit(solution)/shard_map/all_to_all | solution.py:431
  99.8 7.5 %collective-permute-start.20 = (bf16[192,256]{1,0:T(8,128)(2,1)S(1)}, bf16[192,256]{1,0:T(8,128)(2,1)S(1)}, u32[]{:S(2)}, u32[]{:S(2)}) collective-permute-start(bf16[192,256]{1,0:T(8,128)(2,1)S(1)} %get-tuple-element.94), channel_id=1, source_target_pairs={{0,1},{1,2},{2,3},{3,0},{4,5},{5,6},{6,7},{7,4},{8,9},{9,10},{10,1... | collective-permute-start | bytes 294920 | tf_op jit(solution)/shard_map/ppermute | solution.py:252
  99.9 7.4 %collective-permute-start.19 = (bf16[192,256]{1,0:T(8,128)(2,1)S(1)}, bf16[192,256]{1,0:T(8,128)(2,1)S(1)}, u32[]{:S(2)}, u32[]{:S(2)}) collective-permute-start(bf16[192,256]{1,0:T(8,128)(2,1)S(1)} %get-tuple-element.94), channel_id=1, source_target_pairs={{0,2},{1,3},{2,0},{3,1},{4,6},{5,7},{6,4},{7,5},{8,10},{9,11},{10,... | collective-permute-start | bytes 294920 | tf_op jit(solution)/shard_map/ppermute | solution.py:252
  101.1 6.4 %collective-permute-start.18 = (bf16[192,256]{1,0:T(8,128)(2,1)S(1)}, bf16[192,256]{1,0:T(8,128)(2,1)S(1)}, u32[]{:S(2)}, u32[]{:S(2)}) collective-permute-start(bf16[192,256]{1,0:T(8,128)(2,1)S(1)} %get-tuple-element.94), channel_id=1, source_target_pairs={{0,3},{1,0},{2,1},{3,2},{4,7},{5,4},{6,5},{7,6},{8,11},{9,8},{10,9... | collective-permute-start | bytes 294920 | tf_op jit(solution)/shard_map/ppermute | solution.py:252
  125.5 2.3 %collective-permute-start.21 = (bf16[32,32,256]{2,1,0:T(8,128)(2,1)S(1)}, bf16[32,32,256]{2,1,0:T(8,128)(2,1)S(1)}, u32[]{:S(2)}, u32[]{:S(2)}) collective-permute-start(bf16[32,32,256]{2,1,0:T(8,128)(2,1)S(1)} %get-tuple-element.99), channel_id=1, source_target_pairs={{0,4},{4,0},{8,12},{12,8},{16,20},{20,16},{24,28},{28,24},{32,36},... | collective-permute-start | bytes 1572872 | tf_op jit(solution)/shard_map/ppermute | solution.py:464
  126.3 19.0 %collective-permute-start.13 = (bf16[192,2048]{1,0:T(8,128)(2,1)S(1)}, bf16[192,2048]{1,0:T(8,128)(2,1)S(1)}, u32[]{:S(2)}, u32[]{:S(2)}) collective-permute-start(bf16[192,2048]{1,0:T(8,128)(2,1)S(1)} %copy-done.5), channel_id=1, source_target_pairs={{0,3},{1,0},{2,1},{3,2},{4,7},{5,4},{6,5},{7,6},{8,11},{9,8},{10,9... | collective-permute-start | bytes 2359304 | tf_op jit(solution)/shard_map/ppermute | solution.py:252
  126.3 19.9 %collective-permute-start.12 = (bf16[192,2048]{1,0:T(8,128)(2,1)S(1)}, bf16[192,2048]{1,0:T(8,128)(2,1)S(1)}, u32[]{:S(2)}, u32[]{:S(2)}) collective-permute-start(bf16[192,2048]{1,0:T(8,128)(2,1)S(1)} %copy-done.5), channel_id=1, source_target_pairs={{0,1},{1,2},{2,3},{3,0},{4,5},{5,6},{6,7},{7,4},{8,9},{9,10},{10,1... | collective-permute-start | bytes 2359304 | tf_op jit(solution)/shard_map/ppermute | solution.py:252
  128.8 37.5 %all-to-all-start.2 = ((bf16[32,32,256]{2,1,0:T(8,128)(2,1)}), bf16[32,32,256]{2,1,0:T(8,128)(2,1)S(1)}, u32[]{:S(2)}, u32[]{:S(2)}) async-start(bf16[32,32,256]{2,1,0:T(8,128)(2,1)} %add_convert_fusion), calls=%async_computation.2 | async-start | bytes 1048576 | tf_op jit(solution)/shard_map/all_to_all | solution.py:472
  133.6 21.0 %collective-permute-start.25 = (bf16[192,512]{1,0:T(8,128)(2,1)}, bf16[192,512]{1,0:T(8,128)(2,1)S(1)}, u32[]{:S(2)}, u32[]{:S(2)}) collective-permute-start(bf16[192,512]{1,0:T(8,128)(2,1)} %get-tuple-element.125), channel_id=1, source_target_pairs={{0,1},{1,2},{2,3},{3,0},{4,5},{5,6},{6,7},{7,4},{8,9},{9,10},{10,1... | collective-permute-start | bytes 589832 | tf_op jit(solution)/shard_map/ppermute | solution.py:252
  133.7 20.9 %collective-permute-start.24 = (bf16[192,512]{1,0:T(8,128)(2,1)}, bf16[192,512]{1,0:T(8,128)(2,1)S(1)}, u32[]{:S(2)}, u32[]{:S(2)}) collective-permute-start(bf16[192,512]{1,0:T(8,128)(2,1)} %get-tuple-element.125), channel_id=1, source_target_pairs={{0,2},{1,3},{2,0},{3,1},{4,6},{5,7},{6,4},{7,5},{8,10},{9,11},{10,... | collective-permute-start | bytes 589832 | tf_op jit(solution)/shard_map/ppermute | solution.py:252
  136.0 18.6 %collective-permute-start.23 = (bf16[192,512]{1,0:T(8,128)(2,1)}, bf16[192,512]{1,0:T(8,128)(2,1)S(1)}, u32[]{:S(2)}, u32[]{:S(2)}) collective-permute-start(bf16[192,512]{1,0:T(8,128)(2,1)} %get-tuple-element.125), channel_id=1, source_target_pairs={{0,3},{1,0},{2,1},{3,2},{4,7},{5,4},{6,5},{7,6},{8,11},{9,8},{10,9... | collective-permute-start | bytes 589832 | tf_op jit(solution)/shard_map/ppermute | solution.py:252
  146.6 16.5 %copy-start.9 = (bf16[768,256]{1,0:T(8,128)(2,1)S(1)}, bf16[768,256]{1,0:T(8,128)(2,1)}, u32[]{:S(2)}) copy-start(bf16[768,256]{1,0:T(8,128)(2,1)} %get-tuple-element.106) | copy-start | bytes 1179652
  146.7 16.4 %collective-permute-start.14 = (bf16[96,2048]{1,0:T(8,128)(2,1)S(1)}, bf16[96,2048]{1,0:T(8,128)(2,1)S(1)}, u32[]{:S(2)}, u32[]{:S(2)}) collective-permute-start(bf16[96,2048]{1,0:T(8,128)(2,1)S(1)} %get-tuple-element.86), channel_id=1, source_target_pairs={{0,1},{1,2},{2,3},{3,0},{4,5},{5,6},{6,7},{7,4},{8,9},{9,10},{10,1... | collective-permute-start | bytes 1179656 | tf_op jit(solution)/shard_map/ppermute | solution.py:252
  147.0 16.1 %collective-permute-start.15 = (bf16[96,2048]{1,0:T(8,128)(2,1)S(1)}, bf16[96,2048]{1,0:T(8,128)(2,1)S(1)}, u32[]{:S(2)}, u32[]{:S(2)}) collective-permute-start(bf16[96,2048]{1,0:T(8,128)(2,1)S(1)} %get-tuple-element.87), channel_id=1, source_target_pairs={{0,3},{1,0},{2,1},{3,2},{4,7},{5,4},{6,5},{7,6},{8,11},{9,8},{10,9... | collective-permute-start | bytes 1179656 | tf_op jit(solution)/shard_map/ppermute | solution.py:252
  157.0 8.6 %collective-permute-start.26 = (f32[2,256]{1,0:T(2,128)S(1)}, f32[2,256]{1,0:T(2,128)S(1)}, u32[]{:S(2)}, u32[]{:S(2)}) collective-permute-start(f32[2,256]{1,0:T(2,128)S(1)} %slice.42), channel_id=1, source_target_pairs={{4,0},{8,4},{12,8},{16,12},{20,16},{24,20},{28,24},{32,28},{36,32}... | collective-permute-start | bytes 6152 | tf_op jit(solution)/shard_map/ppermute | solution.py:258
  166.4 7.3 %collective-permute-start.22 = (f32[32,256]{1,0:T(8,128)S(1)}, f32[32,256]{1,0:T(8,128)S(1)}, u32[]{:S(2)}, u32[]{:S(2)}) collective-permute-start(f32[32,256]{1,0:T(8,128)S(1)} %convert_reduce_fusion), channel_id=1, source_target_pairs={{0,2},{1,64},{2,134},{3,196},{4,33},{5,97},{6,165},{7,229},{8,10},... | collective-permute-start | bytes 98312 | tf_op jit(solution)/shard_map/ppermute | solution.py:491
